TPU v7x, 512 devices: a whole 4x4x16 slice. The times are simulated.
512 devices in a mesh: sp: 64 (over z, y), tp: 8 (over x, core).
Axes of the slice: x: 4, y: 4, z: 16, core: 2. Of those that a mesh axis runs over, the one named last changes fastest.
Arguments:
- tokens: bfloat16 [4096, 4, 2048], P(('sp', 'tp')), may hold values from -16 to 16
- norm_gain: float32 [2048], replicated, may hold values from 0.1 to 1.9
- w_query: bfloat16 [2048, 2048], P('sp', 'tp'), may hold values from -0.125 to 0.125
- w_forget: bfloat16 [2048, 2048], P('sp', 'tp'), may hold values from -0.125 to 0.125
- w_value: bfloat16 [2048, 2048], P('sp', 'tp'), may hold values from -0.125 to 0.125
- floor_gap: float32 [2048], P('tp'), may hold values from 0 to 0.15, as said below
- head_gain: float32 [2048], P('tp'), may hold values from 0.1 to 1.9
- w_out: bfloat16 [2048, 2048], P('tp', 'sp'), may hold values from -0.125 to 0.125
Outputs:
- mixed: bfloat16 [4096, 4, 2048], P(('sp', 'tp'))
Inputs may be any that keep to these rules, and one draw needn't show every extreme that they name: `floor_gap`: positive, at least 0.5 / 4096 and at most 0.15.
All inputs are finite; a program needn't handle non-finite values.
Results may differ from a plain program's by a relative error of at most 0.014.
Values may be sent and summed in bfloat16 or wider, within the bound.
No kernel may reach another device: no remote copies, remote signals or barrier semaphores. Data moves between devices by JAX's collectives and lax.ppermute only.
A program may use at most 128 MiB of HBM per device.

v0:
```python
import math

import jax
import jax.numpy as jnp
from jax import lax
from jax.experimental import pallas as pl
from jax.experimental.pallas import tpu as pltpu
from jax.sharding import Mesh
from jax.sharding import PartitionSpec as P


KEY_DIM = 128
VAL_DIM = 128
YT = ("y", "x", "c")
LANES = 128

eps_norm = 1e-06
f32 = jnp.float32
bf16 = jnp.bfloat16


def exchanged(value, axis):
    return lax.all_to_all(value, axis, 0, 0, tiled=True)


def call(kernel, out, flops, *args, scratch=()):
    outs = out if isinstance(out, (list, tuple)) else (out,)
    moved = sum(math.prod(a.shape) * jnp.dtype(a.dtype).itemsize for a in (*args, *outs))
    return pl.pallas_call(
        kernel,
        out_shape=out,
        in_specs=[pl.BlockSpec(memory_space=pltpu.SMEM if a.dtype == jnp.int32 else pltpu.VMEM) for a in args],
        out_specs=jax.tree.map(lambda _: pl.BlockSpec(memory_space=pltpu.VMEM), out),
        scratch_shapes=scratch,
        cost_estimate=pl.CostEstimate(flops=flops, bytes_accessed=moved, transcendentals=0),
        compiler_params=pltpu.CompilerParams(vmem_limit_bytes=16 * 1024 * 1024),
    )(*args)


def dot(a, b, dims):
    return lax.dot_general(a, b, (dims, ((), ())), preferred_element_type=f32)


def shuffled(blocks, chunk, source, rows):
    lane = lax.broadcasted_iota(jnp.int32, (rows, LANES), 1)
    result = None
    for j in range(LANES // chunk):
        block, group = source(j)
        shift = ((j - group) * chunk) % LANES
        moved = blocks(block)
        if shift:
            moved = pltpu.roll(moved, shift, 1)
        result = moved if result is None else jnp.where(lane >= j * chunk, moved, result)
    return result


def normalize_kernel(ny, nt, chunk, x_ref, gain_ref, *refs):
    *weight_refs, out_ref, packed_ref, row_ref = refs
    per = LANES // chunk
    pos, seqs, width = x_ref.shape
    at = 0
    for ref in weight_refs:
        for lower in range(0, ref.shape[1], LANES):
            rows = min(chunk, packed_ref.shape[0] - at)
            whole = rows // 8 * 8
            packed_ref[at : at + whole, :] = ref[:whole, lower : lower + LANES]
            if whole < rows:
                packed_ref[at + whole : at + rows, :] = ref[whole:rows, lower : lower + LANES]
            at += rows
    for p in range(pos):
        x = x_ref[p].astype(f32)
        scale = lax.rsqrt(jnp.mean(x * x, axis=-1, keepdims=True) + eps_norm)
        normed = (x * scale * gain_ref[...]).astype(bf16).astype(f32)
        for b in range(width // LANES):
            row_ref[b, pl.ds(p, seqs, stride=pos), :] = normed[:, b * LANES : (b + 1) * LANES]
    part = width // ny
    for y in range(ny):
        for q in range(part // LANES):

            def source(j):
                flat = ((q * per + j) * ny + y) * chunk
                return flat // LANES, (flat % LANES) // chunk

            block = shuffled(lambda b: row_ref[b], chunk, source, pos * seqs).astype(bf16)
            for t in range(nt):
                out_ref[y, t, :, q * LANES : (q + 1) * LANES] = block


def split_parts(value):
    first = value.astype(bf16)
    rest = value - first.astype(f32)
    second = rest.astype(bf16)
    third = (rest - second.astype(f32)).astype(bf16)
    return first, second, third


def joined(weights_ref, chunk, which):
    nz, _, lanes = weights_ref.shape
    halves = []
    for half in range(2):
        at = (2 * which + half) * chunk
        halves.append(weights_ref[:, at : at + chunk, :].reshape(nz * chunk, lanes))
    return jnp.concatenate(halves, axis=1)


def first_projection_kernel(rows_ref, weights_ref, out_t_ref, fv_ref):
    seqs = fv_ref.shape[0]
    sources, _, pos, part = rows_ref.shape
    stretch = sources * pos
    chunk, width = out_t_ref.shape
    rest = pltpu.roll(out_t_ref[chunk - 8 :, LANES:].astype(f32), 2, 0)
    rest = jnp.concatenate([rest, jnp.zeros((8, fv_ref.shape[2] - LANES), f32)], axis=1).astype(bf16)
    both = [joined(weights_ref, chunk, k) for k in range(2)]
    for s in range(seqs):
        rows = rows_ref[:, s].reshape(stretch, part)
        for k in range(2):
            fv_ref[s, :stretch, k * width : (k + 1) * width] = dot(rows, both[k], ((1,), (0,))).astype(bf16)
        fv_ref[s, stretch:, :] = rest


def put_out_rows(weights_ref, chunk, ref, base):
    nz = weights_ref.shape[0]
    first, second = 6 * chunk, 7 * chunk
    whole = chunk - 8
    for z in range(nz):
        at = base + z * chunk
        ref[at : at + chunk, :LANES] = weights_ref[z, first:second, :]
        ref[at : at + whole, LANES:] = weights_ref[z, second : second + whole, :]
        ref[at + whole : at + chunk, LANES:] = jnp.zeros((8, LANES), bf16)
        ref[at + whole : at + whole + 6, LANES:] = weights_ref[z, second + whole : second + whole + 6, :]


def second_projection_kernel(rows_ref, weights_ref, *out_refs):
    ny = len(out_refs)
    sources, _, pos, part = rows_ref.shape
    stretch = sources * pos
    chunk = part // weights_ref.shape[0]
    query = joined(weights_ref, chunk, 2)
    for d in range(ny):
        rows = rows_ref[:, lax.rem(lax.axis_index("y") + d, ny)].reshape(stretch, part)
        out_refs[d][:stretch, :] = dot(rows, query, ((1,), (0,))).astype(bf16)
        if out_refs[d].shape[0] > stretch:
            put_out_rows(weights_ref, chunk, out_refs[d], stretch)


def far_rows_kernel(chunk, weights_ref, far_ref):
    put_out_rows(weights_ref, chunk, far_ref, 0)


def whole_out_rows(ref, base, piece_ref, d, out_ref):
    nz, chunk, _ = out_ref.shape
    edge_row = lax.broadcasted_iota(jnp.int32, (8, LANES), 0)
    rest_at = piece_ref.shape[1] - 8
    for z in range(nz):
        at = base + z * chunk
        out_ref[z, :, :LANES] = ref[at : at + chunk, :LANES]
        out_ref[z, : chunk - 8, LANES:] = ref[at : at + chunk - 8, LANES:]
        moved = pltpu.roll(piece_ref[z, rest_at:, :].astype(f32), (6 - 2 * d) % 8, 0)
        old = ref[at + chunk - 8 : at + chunk, LANES:].astype(f32)
        out_ref[z, chunk - 8 :, LANES:] = jnp.where(edge_row >= 6, moved, old).astype(bf16)


def gates_kernel(fv_ref, gap_ref, piece_ref, sums_ref, inkey_ref, values_ref):
    ny = fv_ref.shape[0]
    stretch, width = sums_ref.shape
    nz = piece_ref.shape[0]
    mine = width // nz

    def total(lower):
        result = fv_ref[0, :stretch, lower : lower + width].astype(f32)
        for k in range(1, ny):
            result = result + fv_ref[k, :stretch, lower : lower + width].astype(f32)
        return result.astype(bf16)

    forget = total(0).astype(f32)
    values = total(width)
    values_ref[...] = values
    inkey = gap_ref[...] * jax.nn.sigmoid(-forget)
    log_forget = jnp.log1p(-inkey)
    row = lax.broadcasted_iota(jnp.int32, (stretch, stretch), 0)
    column = lax.broadcasted_iota(jnp.int32, (stretch, stretch), 1)
    causal = (row >= column).astype(bf16)
    parts = split_parts(log_forget)
    cumulative = sum(dot(causal, p, ((1,), (0,))) for p in parts)
    final = cumulative[stretch - 1 : stretch, :]
    sums_ref[...] = cumulative
    inkey_ref[...] = inkey
    key_final = (inkey * jnp.exp(final - cumulative)).astype(bf16)
    ones = jnp.ones((stretch, LANES), bf16)
    lane = lax.broadcasted_iota(jnp.int32, (8, LANES), 1)
    row = lax.broadcasted_iota(jnp.int32, (8, LANES), 0)
    rests = jnp.zeros((8, LANES), f32)
    for d in range(ny):
        source = lax.rem(lax.axis_index("y") + ny - d, ny)
        moved = fv_ref[source, stretch:, :LANES].astype(f32)
        rests = jnp.where(row // 2 == d, pltpu.roll(moved, 2 * d, 0) if d else moved, rests)
    rests = rests.astype(bf16)
    per_head = KEY_DIM // mine
    for h in range(width // KEY_DIM):
        cut = slice(h * KEY_DIM, (h + 1) * KEY_DIM)
        state = dot(key_final[:, cut], values[:, cut], ((0,), (0,))).astype(bf16)
        decay = jnp.exp(sum(dot(p[:, cut], ones, ((0,), (0,))) for p in parts))
        high = decay.astype(bf16).astype(f32)
        low = (decay - high).astype(bf16).astype(f32)
        for k in range(per_head):
            at = h * per_head + k
            lower = k * mine
            piece_ref[at, :mine, :] = state[lower : lower + mine]
            top = jnp.where(lane < 32, high[lower : lower + 8], low[lower : lower + 8])
            bottom = jnp.where(lane < 96, high[lower + 8 : lower + 16], low[lower + 8 : lower + 16])
            piece_ref[at, mine : mine + 8, :] = jnp.where(lane < 64, top, bottom).astype(bf16)
            piece_ref[at, mine + 8 :, :] = rests


def keys_kernel(sums_ref, inkey_ref, keys_ref):
    keys_ref[...] = (inkey_ref[...] * jnp.exp(-sums_ref[...])).astype(bf16)


def reach_kernel(sums_ref, reach_ref):
    reach_ref[...] = jnp.exp(sums_ref[...])


def prefix_kernel(piece_ref, out_ref):
    nz, mine, _ = out_ref.shape
    state = [jnp.zeros((8, VAL_DIM), f32) for _ in range(2)]
    for k in range(nz):
        out_ref[k] = jnp.concatenate(state, axis=0).astype(bf16)
        packed = piece_ref[k, mine : mine + 8, :].astype(f32)
        added = piece_ref[k, :mine, :].astype(f32)
        for i in range(2):
            factor = packed[:, 64 * i : 64 * i + 1] + packed[:, 64 * i + 32 : 64 * i + 33]
            state[i] = factor * state[i] + added[8 * i : 8 * i + 8]


def inside_kernel(*refs):
    *later_refs, reach_ref, keys_ref, values_ref, piece_ref, inside_ref, out_t_ref = refs
    stretch, width = reach_ref.shape
    query = later_refs[0][:stretch, :].astype(f32)
    for ref in later_refs[1:]:
        query = query + ref[:stretch, :].astype(f32)
    query = jax.nn.silu(query.astype(bf16).astype(f32))
    scaled = (query * reach_ref[...]).astype(bf16)
    inside_ref[:, width:] = scaled.astype(f32)
    row = lax.broadcasted_iota(jnp.int32, (stretch, stretch), 0)
    column = lax.broadcasted_iota(jnp.int32, (stretch, stretch), 1)
    causal = row >= column
    for h in range(width // KEY_DIM):
        cut = slice(h * KEY_DIM, (h + 1) * KEY_DIM)
        scores = dot(scaled[:, cut], keys_ref[:, cut], ((1,), (1,)))
        scores = jnp.where(causal, scores, 0.0).astype(bf16)
        inside_ref[:, cut] = dot(scores, values_ref[:, cut], ((1,), (0,)))
    for d, ref in enumerate(later_refs):
        if ref.shape[0] > stretch:
            whole_out_rows(ref, stretch, piece_ref, d, out_t_ref.at[d])


def merge_kernel(far, far_ref, piece_ref, out_ref):
    whole_out_rows(far_ref, 0, piece_ref, far, out_ref)


def readout_kernel(far, inside_ref, out_t_ref, far_out_ref, state_ref, gain_ref, give_ref, keep_ref):
    ny, nz, chunk, width = out_t_ref.shape
    stretch = inside_ref.shape[0]
    scaled = inside_ref[:, width:].astype(bf16)
    hidden = []
    for h in range(width // KEY_DIM):
        cut = slice(h * KEY_DIM, (h + 1) * KEY_DIM)
        recurrent = inside_ref[:, cut] + dot(scaled[:, cut], state_ref[cut, :], ((1,), (0,)))
        mean_square = jnp.mean(recurrent * recurrent, axis=-1, keepdims=True)
        hidden.append(recurrent * lax.rsqrt(mean_square + eps_norm) * gain_ref[:, cut])
    half = stretch // 2
    hidden = jnp.concatenate(hidden, axis=1).reshape(stretch // 16, 2, 8, width)
    first, second = (hidden[:, k].reshape(half, width) for k in range(2))
    at_first = lax.axis_index("c") == 0
    hidden = jnp.concatenate([jnp.where(at_first, second, first), jnp.where(at_first, first, second)], axis=0)
    hidden = hidden.astype(bf16)
    part = nz * chunk
    for d in range(ny):
        weight = (far_out_ref[...] if d == far else out_t_ref[d]).reshape(part, width)
        source = lax.rem(lax.axis_index("y") + ny - d, ny)
        columns = pl.ds(pl.multiple_of(source * part, part), part)
        mixed = dot(hidden, weight, ((1,), (1,))).astype(bf16)
        give_ref[:, columns] = mixed[:half]
        keep_ref[:, columns] = mixed[half:]


def pair_kernel(kept_ref, given_ref, out_ref):
    out_ref[...] = (kept_ref[...].astype(f32) + given_ref[...].astype(f32)).astype(bf16)


def gather_kernel(nz, chunk, in_ref, out_ref, row_ref):
    seqs, nt, pos, width = in_ref.shape
    ny = width // (nz * chunk)
    part = nz * chunk
    per = LANES // chunk
    for s in range(seqs):
        summed = in_ref[s, 0].astype(f32)
        for t in range(1, nt):
            summed = summed + in_ref[s, t].astype(f32)
        for b in range(width // LANES):

            def source(j):
                z, y = divmod(b * per + j, ny)
                flat = y * part + z * chunk
                return flat // LANES, (flat % LANES) // chunk

            block = shuffled(lambda k: summed[:, k * LANES : (k + 1) * LANES], chunk, source, pos)
            row_ref[b, s * pos : (s + 1) * pos, :] = block
    for p in range(pos):
        for b in range(width // LANES):
            rows = row_ref[b, pl.ds(p, seqs, stride=pos), :].astype(bf16)
            out_ref[p, :, b * LANES : (b + 1) * LANES] = rows


def block(tokens, norm_gain, w_query, w_forget, w_value, floor_gap, head_gain, w_out):
    nz, ny, nx, nc = (lax.axis_size(a) for a in ("z", "y", "x", "c"))
    nt = nx * nc
    pos, seqs, width = tokens.shape
    chunk, key_width = w_query.shape
    stretch = pos * ny * nt
    part = nz * chunk
    shape = jax.ShapeDtypeStruct

    out_t = w_out.T
    send, packed = call(
        lambda *refs: normalize_kernel(ny, nt, chunk, *refs),
        [
            pltpu.HBM((ny, nt, seqs * pos, part), bf16),
            shape((8 * chunk - 2, LANES), bf16),
        ],
        1_000_000,
        *(
            pltpu.with_memory_space_constraint(value, pltpu.MemorySpace.HBM)
            for value in (tokens, norm_gain.reshape(1, width), w_forget, w_value, w_query, out_t)
        ),
        scratch=[pltpu.VMEM((width // LANES, seqs * pos, LANES), f32)],
    )
    rows = exchanged(send.reshape(ny * nt, seqs, pos, part), YT)

    weights = lax.all_gather(packed, "z", axis=0)
    mine = key_width // nz
    far = ny // 2

    fv = call(
        first_projection_kernel, shape((seqs, stretch + 8, 2 * key_width), bf16), 550_000_000, rows, weights, out_t
    )
    fv = exchanged(fv, "y")
    pieces, sums, inkey, values = call(
        gates_kernel,
        [
            pltpu.HBM((nz, mine + 16, VAL_DIM), bf16),
            shape((stretch, key_width), f32),
            shape((stretch, key_width), f32),
            shape((stretch, key_width), bf16),
        ],
        100_000_000,
        fv,
        floor_gap.reshape(1, key_width),
    )
    pieces = exchanged(pieces, "z")
    sent = call(
        second_projection_kernel,
        [pltpu.HBM((stretch + (part if d != far else 0), key_width), bf16) for d in range(ny)],
        280_000_000,
        rows,
        weights,
    )

    def shifted(value, d):
        return lax.ppermute(value, "y", [(i, (i + d) % ny) for i in range(ny)])

    later = [sent[0]] + [shifted(sent[d], d) for d in range(1, ny)]
    far_out = call(lambda *refs: far_rows_kernel(chunk, *refs), pltpu.HBM((part, key_width), bf16), 1_000_000, weights)
    far_out = shifted(far_out, far)
    keys = call(keys_kernel, shape((stretch, key_width), bf16), 1_000_000, sums, inkey)
    reach = call(reach_kernel, shape((stretch, key_width), f32), 1_000_000, sums)
    entering = call(prefix_kernel, shape((nz, mine, VAL_DIM), bf16), 1_000_000, pieces)
    incoming = exchanged(entering, "z").reshape(key_width, VAL_DIM)
    inside, whole_out = call(
        inside_kernel,
        [
            shape((stretch, 2 * key_width), f32),
            shape((ny, nz, chunk, key_width), bf16),
        ],
        100_000_000,
        *later,
        reach,
        keys,
        values,
        pieces,
    )
    far_out = call(
        lambda *refs: merge_kernel(far, *refs), shape((nz, chunk, key_width), bf16), 1_000_000, far_out, pieces
    )
    give, kept = call(
        lambda *refs: readout_kernel(far, *refs),
        [pltpu.HBM((stretch // 2, width), bf16), shape((stretch // 2, width), bf16)],
        300_000_000,
        inside,
        whole_out,
        far_out,
        incoming,
        head_gain.reshape(1, key_width),
    )
    given = lax.ppermute(give, "c", [(0, 1), (1, 0)])
    mixed = call(pair_kernel, shape((stretch // 2, width), bf16), 1_000_000, kept, given)
    mixed = exchanged(mixed.reshape(ny * nx, pos, width), ("y", "x"))
    mixed = call(
        lambda *refs: gather_kernel(nz, chunk, *refs),
        shape((pos, seqs, width), bf16),
        1_000_000,
        mixed.reshape(seqs, nx, pos, width),
        scratch=[pltpu.VMEM((width // LANES, seqs * pos, LANES), f32)],
    )
    return mixed


def solution(mesh):
    finer = Mesh(mesh.devices.reshape(16, 4, 4, 2), ("z", "y", "x", "c"))
    sp, tp = ("z", "y"), ("x", "c")
    in_specs = (
        P((*sp, *tp), None, None),
        P(),
        P(sp, tp),
        P(sp, tp),
        P(sp, tp),
        P(tp),
        P(tp),
        P(tp, sp),
    )
    out_specs = P((*sp, *tp), None, None)
    return jax.shard_map(block, mesh=finer, in_specs=in_specs, out_specs=out_specs, check_vma=False)
```

profile of v0, /device:TPU:1, one launch (start us, length us, event | category | flops | bytes accessed | tf_op | source)
XLA Modules:
  0.0 139.4 jit_solution(6403400004805874268)
XLA Ops:
  0.0 2.4 %shard_map.82 = (bf16[4,8,32,512]{3,2,1,0:T(8,128)(2,1)}, bf16[254,128]{1,0:T(8,128)(2,1)S(1)}) custom-call(bf16[8,4,2048]{2,1,0:T(4,128)(2,1)} %refs_0_.1, f32[1,2048]{1,0:T(1,128)} %bitcast.18, bf16[32,256]{1,0:T(8,128)(2,1)} %refs_2_.1, bf16[32,256]{1,0:T(8,128)(2,1)} %refs_3_.1, bf16[32,256]{1,0:T(8,128)(2,1)} %refs_4_.1, bf16[32,256]{1,0:T(8,128)(2,1)} %bitcast.12), custom_call_target="tpu_custom_call" | custom-call | flops 1000000 | bytes 1318400 | tf_op jit(solution)/shard_map/pallas_call | solution.py:29
  2.4 10.4 %all-to-all-start = ((bf16[32,4,8,512]{3,2,1,0:T(8,128)(2,1)}), bf16[32,4,8,512]{3,2,1,0:T(8,128)(2,1)S(1)}, u32[]{:S(2)}, u32[]{:S(2)}) async-start(bf16[32,4,8,512]{3,2,1,0:T(8,128)(2,1)} %bitcast.17), calls=%async_computation | async-start | bytes 2097152 | tf_op jit(solution)/shard_map/all_to_all | solution.py:23
  12.8 0.0 copy-start.5
  12.8 33.6 %all-gather.1.weights_ref.refs_0_ = bf16[16,254,128]{2,1,0:T(8,128)(2,1)S(1)} all-gather(bf16[1,254,128]{2,1,0:T(8,128)(2,1)S(1)} %bitcast.14), channel_id=2, replica_groups=mesh['z'=16,'y'=4,'x'=4,'c'=2] {'z'}, dimensions={0}, use_global_device_ids=true | all-gather | bytes 1105408 | tf_op jit(solution)/shard_map/all_gather | solution.py:340
  46.5 0.0 all-to-all-done.rows_ref
  46.5 0.0 copy-done.5
  46.5 0.7 shard_map.84
  47.2 0.0 copy-start.7
  47.2 14.1 %all_to_all.25.fv_ref = bf16[4,264,512]{2,1,0:T(8,128)(2,1)S(1)} all-to-all(bf16[4,264,512]{2,1,0:T(8,128)(2,1)S(1)} %shard_map.84), channel_id=1, replica_groups=mesh['z'=16,'y'=4,'x'=4,'c'=2] {'y'}, dimensions={0} | all-to-all | bytes 2162688 | tf_op jit(solution)/shard_map/all_to_all | solution.py:23
  61.3 0.0 copy-done.7
  61.3 1.7 %shard_map.85 = (bf16[16,32,128]{2,1,0:T(8,128)(2,1)}, f32[256,256]{1,0:T(8,128)S(1)}, f32[256,256]{1,0:T(8,128)S(1)}, bf16[256,256]{1,0:T(8,128)(2,1)S(1)}) custom-call(bf16[4,264,512]{2,1,0:T(8,128)(2,1)S(1)} %all_to_all.25.fv_ref, f32[1,256]{1,0:T(1,128)S(1)} %bitcast.16), custom_call_target="tpu_custom_call" | custom-call | flops 100000000 | bytes 1868800 | tf_op jit(solution)/shard_map/pallas_call | solution.py:29
  63.0 0.0 copy-start.3
  63.0 0.7 copy-done.3
  63.7 7.0 %all-to-all-start.2 = ((bf16[16,32,128]{2,1,0:T(8,128)(2,1)}), bf16[16,32,128]{2,1,0:T(8,128)(2,1)S(1)}, u32[]{:S(2)}, u32[]{:S(2)}) async-start(bf16[16,32,128]{2,1,0:T(8,128)(2,1)} %get-tuple-element.28), calls=%async_computation.2 | async-start | bytes 262144 | tf_op jit(solution)/shard_map/all_to_all | solution.py:23
  70.7 1.5 %shard_map.83 = (bf16[768,256]{1,0:T(8,128)(2,1)}, bf16[768,256]{1,0:T(8,128)(2,1)}, bf16[256,256]{1,0:T(8,128)(2,1)}, bf16[768,256]{1,0:T(8,128)(2,1)}) custom-call(bf16[32,4,8,512]{3,2,1,0:T(8,128)(2,1)S(1)} %all-to-all-done.rows_ref, bf16[16,254,128]{2,1,0:T(8,128)(2,1)S(1)} %all-gather.1.weights_ref.refs_0_), custom_call_target="tpu_custom_call" | custom-call | flops 280000000 | bytes 3399680 | tf_op jit(solution)/shard_map/pallas_call | solution.py:29
  72.2 0.0 copy-start.8
  72.2 2.3 %collective-permute-start = (bf16[768,256]{1,0:T(8,128)(2,1)}, bf16[768,256]{1,0:T(8,128)(2,1)S(1)}, u32[]{:S(2)}, u32[]{:S(2)}) collective-permute-start(bf16[768,256]{1,0:T(8,128)(2,1)} %get-tuple-element.22), channel_id=1, source_target_pairs={{0,8},{8,16},{16,24},{24,0},{1,9},{9,17},{17,25},{25,1},{2,10},{10... | collective-permute-start | bytes 1179656 | tf_op jit(solution)/shard_map/ppermute | solution.py:370
  74.5 0.0 copy-start.4
  74.5 4.4 %collective-permute-start.2 = (bf16[768,256]{1,0:T(8,128)(2,1)}, bf16[768,256]{1,0:T(8,128)(2,1)S(1)}, u32[]{:S(2)}, u32[]{:S(2)}) collective-permute-start(bf16[768,256]{1,0:T(8,128)(2,1)} %get-tuple-element.24), channel_id=1, source_target_pairs={{0,24},{8,0},{16,8},{24,16},{1,25},{9,1},{17,9},{25,17},{2,26},{10... | collective-permute-start | bytes 1179656 | tf_op jit(solution)/shard_map/ppermute | solution.py:370
  79.0 0.8 shard_map.89
  79.7 0.0 copy-start
  79.7 2.0 %collective-permute-start.3 = (bf16[512,256]{1,0:T(8,128)(2,1)}, bf16[512,256]{1,0:T(8,128)(2,1)S(1)}, u32[]{:S(2)}, u32[]{:S(2)}) collective-permute-start(bf16[512,256]{1,0:T(8,128)(2,1)} %shard_map.89), channel_id=1, source_target_pairs={{0,16},{8,24},{16,0},{24,8},{1,17},{9,25},{17,1},{25,9},{2,18},{10... | collective-permute-start | bytes 786440 | tf_op jit(solution)/shard_map/ppermute | solution.py:370
  81.8 1.0 all-to-all-done.2.refs_7_.refs_1_.piece_ref
  82.7 0.8 shard_map.91
  83.6 10.5 %all-to-all-start.3 = ((bf16[16,16,128]{2,1,0:T(8,128)(2,1)}), bf16[16,16,128]{2,1,0:T(8,128)(2,1)S(1)}, u32[]{:S(2)}, u32[]{:S(2)}) async-start(bf16[16,16,128]{2,1,0:T(8,128)(2,1)} %shard_map.91), calls=%async_computation.3 | async-start | bytes 131072 | tf_op jit(solution)/shard_map/all_to_all | solution.py:23
  94.1 0.0 copy-done.8
  94.1 4.9 %collective-permute-start.1 = (bf16[256,256]{1,0:T(8,128)(2,1)S(1)}, bf16[256,256]{1,0:T(8,128)(2,1)S(1)}, u32[]{:S(2)}, u32[]{:S(2)}) collective-permute-start(bf16[256,256]{1,0:T(8,128)(2,1)S(1)} %copy-done.8), channel_id=1, source_target_pairs={{0,16},{8,24},{16,0},{24,8},{1,17},{9,25},{17,1},{25,9},{2,18},{10... | collective-permute-start | bytes 393224 | tf_op jit(solution)/shard_map/ppermute | solution.py:370
  99.0 0.0 copy-done.4
  99.1 0.0 collective-permute-done.3.refs_0_
  99.1 0.0 copy-start.6
  99.1 2.2 %collective-permute-done.1.refs_2_ = bf16[256,256]{1,0:T(8,128)(2,1)S(1)} collective-permute-done((bf16[256,256]{1,0:T(8,128)(2,1)S(1)}, bf16[256,256]{1,0:T(8,128)(2,1)S(1)}, u32[]{:S(2)}, u32[]{:S(2)}) %collective-permute-start.1) | collective-permute-done | bytes 131104 | tf_op jit(solution)/shard_map/ppermute | solution.py:370
  101.3 0.0 collective-permute-done.refs_1_
  101.3 0.0 collective-permute-done.2.refs_3_
  101.3 0.0 copy-start.1
  101.3 0.7 copy-done.1
  102.1 0.0 copy-done
  102.1 0.0 copy-start.2
  102.1 1.0 copy-done.2
  103.1 0.5 shard_map.88
  103.6 2.1 %all-to-all-done.3 = bf16[16,16,128]{2,1,0:T(8,128)(2,1)S(1)} async-done(((bf16[16,16,128]{2,1,0:T(8,128)(2,1)}), bf16[16,16,128]{2,1,0:T(8,128)(2,1)S(1)}, u32[]{:S(2)}, u32[]{:S(2)}) %all-to-all-start.3) | async-done | bytes 65568 | tf_op jit(solution)/shard_map/all_to_all | solution.py:23
  105.6 0.0 copy-done.6
  105.6 1.4 %shard_map.92 = (bf16[128,2048]{1,0:T(8,128)(2,1)}, bf16[128,2048]{1,0:T(8,128)(2,1)S(1)}) custom-call(f32[256,512]{1,0:T(8,128)S(1)} %get-tuple-element.29.refs_0_, bf16[4,16,32,256]{3,2,1,0:T(8,128)(2,1)S(1)} %get-tuple-element.30.refs_1_, bf16[16,32,256]{2,1,0:T(8,128)(2,1)S(1)} %shard_map.90.refs_2_, bf16[256,128]{1,0:T(8,128)(2,1)S(1)} %bitcast.11, ...), custom_call_target="tpu_custom_call" | custom-call | flops 300000000 | bytes 2950144 | tf_op jit(solution)/shard_map/pallas_call | solution.py:29
  107.1 11.8 %collective-permute-start.4 = (bf16[128,2048]{1,0:T(8,128)(2,1)}, bf16[128,2048]{1,0:T(8,128)(2,1)S(1)}, u32[]{:S(2)}, u32[]{:S(2)}) collective-permute-start(bf16[128,2048]{1,0:T(8,128)(2,1)} %get-tuple-element.32), channel_id=1, source_target_pairs={{0,1},{1,0},{2,3},{3,2},{4,5},{5,4},{6,7},{7,6},{8,9},{9,8},{10,11... | collective-permute-start | bytes 1572872 | tf_op jit(solution)/shard_map/ppermute | solution.py:405
  118.9 1.7 %collective-permute-done.4.given_ref = bf16[128,2048]{1,0:T(8,128)(2,1)S(1)} collective-permute-done((bf16[128,2048]{1,0:T(8,128)(2,1)}, bf16[128,2048]{1,0:T(8,128)(2,1)S(1)}, u32[]{:S(2)}, u32[]{:S(2)}) %collective-permute-start.4) | collective-permute-done | bytes 524320 | tf_op jit(solution)/shard_map/ppermute | solution.py:405
  120.6 0.1 shard_map.93
  120.7 17.7 %all_to_all.26 = bf16[16,8,2048]{2,1,0:T(8,128)(2,1)S(1)} all-to-all(bf16[16,8,2048]{2,1,0:T(8,128)(2,1)S(1)} %bitcast.9), channel_id=1, replica_groups=mesh['z'=16,'y'=4,'x'=4,'c'=2] {'y','x'}, dimensions={0} | all-to-all | bytes 1048576 | tf_op jit(solution)/shard_map/all_to_all | solution.py:23
  138.4 1.0 shard_map.94
  (3 shorter events, 0.1 us)
Async XLA Ops:
  2.4 44.1 %all-to-all-start = ((bf16[32,4,8,512]{3,2,1,0:T(8,128)(2,1)}), bf16[32,4,8,512]{3,2,1,0:T(8,128)(2,1)S(1)}, u32[]{:S(2)}, u32[]{:S(2)}) async-start(bf16[32,4,8,512]{3,2,1,0:T(8,128)(2,1)} %bitcast.17), calls=%async_computation | async-start | bytes 2097152 | tf_op jit(solution)/shard_map/all_to_all | solution.py:23
  12.8 33.7 %copy-start.5 = (bf16[256,32]{0,1:T(8,128)(2,1)S(1)}, bf16[256,32]{0,1:T(8,128)(2,1)}, u32[]{:S(2)}) copy-start(bf16[256,32]{0,1:T(8,128)(2,1)} %param.15) | copy-start | bytes 49156
  47.2 14.1 %copy-start.7 = (f32[256]{0:T(256)S(1)}, f32[256]{0:T(256)}, u32[]{:S(2)}) copy-start(f32[256]{0:T(256)} %param.13) | copy-start | bytes 3076
  63.0 0.7 copy-start.3
  63.7 19.0 %all-to-all-start.2 = ((bf16[16,32,128]{2,1,0:T(8,128)(2,1)}), bf16[16,32,128]{2,1,0:T(8,128)(2,1)S(1)}, u32[]{:S(2)}, u32[]{:S(2)}) async-start(bf16[16,32,128]{2,1,0:T(8,128)(2,1)} %get-tuple-element.28), calls=%async_computation.2 | async-start | bytes 262144 | tf_op jit(solution)/shard_map/all_to_all | solution.py:23
  72.2 21.9 %copy-start.8 = (bf16[256,256]{1,0:T(8,128)(2,1)S(1)}, bf16[256,256]{1,0:T(8,128)(2,1)}, u32[]{:S(2)}) copy-start(bf16[256,256]{1,0:T(8,128)(2,1)} %get-tuple-element.23) | copy-start | bytes 393220
  72.2 29.1 %collective-permute-start = (bf16[768,256]{1,0:T(8,128)(2,1)}, bf16[768,256]{1,0:T(8,128)(2,1)S(1)}, u32[]{:S(2)}, u32[]{:S(2)}) collective-permute-start(bf16[768,256]{1,0:T(8,128)(2,1)} %get-tuple-element.22), channel_id=1, source_target_pairs={{0,8},{8,16},{16,24},{24,0},{1,9},{9,17},{17,25},{25,1},{2,10},{10... | collective-permute-start | bytes 1179656 | tf_op jit(solution)/shard_map/ppermute | solution.py:370
  74.5 24.5 %copy-start.4 = (f32[256,256]{1,0:T(8,128)S(1)}, f32[256,256]{1,0:T(8,128)}, u32[]{:S(2)}) copy-start(f32[256,256]{1,0:T(8,128)} %copy-done.3) | copy-start | bytes 786436
  74.5 26.8 %collective-permute-start.2 = (bf16[768,256]{1,0:T(8,128)(2,1)}, bf16[768,256]{1,0:T(8,128)(2,1)S(1)}, u32[]{:S(2)}, u32[]{:S(2)}) collective-permute-start(bf16[768,256]{1,0:T(8,128)(2,1)} %get-tuple-element.24), channel_id=1, source_target_pairs={{0,24},{8,0},{16,8},{24,16},{1,25},{9,1},{17,9},{25,17},{2,26},{10... | collective-permute-start | bytes 1179656 | tf_op jit(solution)/shard_map/ppermute | solution.py:370
  79.7 22.3 %copy-start = (bf16[768,256]{1,0:T(8,128)(2,1)S(1)}, bf16[768,256]{1,0:T(8,128)(2,1)}, u32[]{:S(2)}) copy-start(bf16[768,256]{1,0:T(8,128)(2,1)} %get-tuple-element.21.refs_0_) | copy-start | bytes 1179652
  79.7 19.4 %collective-permute-start.3 = (bf16[512,256]{1,0:T(8,128)(2,1)}, bf16[512,256]{1,0:T(8,128)(2,1)S(1)}, u32[]{:S(2)}, u32[]{:S(2)}) collective-permute-start(bf16[512,256]{1,0:T(8,128)(2,1)} %shard_map.89), channel_id=1, source_target_pairs={{0,16},{8,24},{16,0},{24,8},{1,17},{9,25},{17,1},{25,9},{2,18},{10... | collective-permute-start | bytes 786440 | tf_op jit(solution)/shard_map/ppermute | solution.py:370
  83.6 22.1 %all-to-all-start.3 = ((bf16[16,16,128]{2,1,0:T(8,128)(2,1)}), bf16[16,16,128]{2,1,0:T(8,128)(2,1)S(1)}, u32[]{:S(2)}, u32[]{:S(2)}) async-start(bf16[16,16,128]{2,1,0:T(8,128)(2,1)} %shard_map.91), calls=%async_computation.3 | async-start | bytes 131072 | tf_op jit(solution)/shard_map/all_to_all | solution.py:23
  94.1 7.2 %collective-permute-start.1 = (bf16[256,256]{1,0:T(8,128)(2,1)S(1)}, bf16[256,256]{1,0:T(8,128)(2,1)S(1)}, u32[]{:S(2)}, u32[]{:S(2)}) collective-permute-start(bf16[256,256]{1,0:T(8,128)(2,1)S(1)} %copy-done.8), channel_id=1, source_target_pairs={{0,16},{8,24},{16,0},{24,8},{1,17},{9,25},{17,1},{25,9},{2,18},{10... | collective-permute-start | bytes 393224 | tf_op jit(solution)/shard_map/ppermute | solution.py:370
  99.1 6.5 %copy-start.6 = (f32[256]{0:T(256)S(1)}, f32[256]{0:T(256)}, u32[]{:S(2)}) copy-start(f32[256]{0:T(256)} %param.14) | copy-start | bytes 3076
  101.3 0.7 copy-start.1
  102.1 1.0 copy-start.2
  107.1 13.5 %collective-permute-start.4 = (bf16[128,2048]{1,0:T(8,128)(2,1)}, bf16[128,2048]{1,0:T(8,128)(2,1)S(1)}, u32[]{:S(2)}, u32[]{:S(2)}) collective-permute-start(bf16[128,2048]{1,0:T(8,128)(2,1)} %get-tuple-element.32), channel_id=1, source_target_pairs={{0,1},{1,0},{2,3},{3,2},{4,5},{5,4},{6,7},{7,6},{8,9},{9,8},{10,11... | collective-permute-start | bytes 1572872 | tf_op jit(solution)/shard_map/ppermute | solution.py:405
where the time goes:
time: 140 us; the launch traced here: 139 us
  blocking collectives  65.5 us (47%)
  starting transfers between devices  53.3 us (38%)
  Pallas kernels  11 us (8%)
  waiting for transfers between devices  6.94 us (5%)
  local copies, waits for them, and re-layouts  2.47 us (2%)
    all_gather x1, blocking collectives, block(): weights = lax.all_gather(packed, 'z', axis=0)  33.6 us
    all_to_all x2, blocking collectives, exchanged(): return lax.all_to_all(value, axis, 0, 0, tiled=True)  31.8 us
    all_to_all x3, starting transfers between devices, exchanged(): return lax.all_to_all(value, axis, 0, 0, tiled=True)  27.9 us
    ppermute x4, starting transfers between devices, shifted(): return lax.ppermute(value, 'y', [(i, (i + d) % ny) for i in range(ny)])  13.6 us
    ppermute x1, starting transfers between devices, block(): given = lax.ppermute(give, 'c', [(0, 1), (1, 0)])  11.8 us
    pallas_call x13, Pallas kernels, call(): pl.pallas_call(kernel, out_shape=out, in_specs=[pl.BlockSpec(memory_space...  11 us
    all_to_all x3, waiting for transfers between devices, exchanged(): return lax.all_to_all(value, axis, 0, 0, tiled=True)  3.04 us
  transfers between devices with their start and end apart: 8, of which 4 were waited for; matrix products, arithmetic and copies ran while one was open for 0% of the time, Pallas kernels for 3%

commit v1 on v0

--- a/solution.py
+++ b/solution.py
@@ -23,14 +23,15 @@
     return lax.all_to_all(value, axis, 0, 0, tiled=True)
 
 
-def call(kernel, out, flops, *args, scratch=()):
+def call(kernel, out, flops, *args, scratch=(), copied=()):
     outs = out if isinstance(out, (list, tuple)) else (out,)
     moved = sum(math.prod(a.shape) * jnp.dtype(a.dtype).itemsize for a in (*args, *outs))
+    specs = [pl.BlockSpec(memory_space=pl.ANY if i in copied else pltpu.VMEM) for i in range(len(outs))]
     return pl.pallas_call(
         kernel,
         out_shape=out,
         in_specs=[pl.BlockSpec(memory_space=pltpu.SMEM if a.dtype == jnp.int32 else pltpu.VMEM) for a in args],
-        out_specs=jax.tree.map(lambda _: pl.BlockSpec(memory_space=pltpu.VMEM), out),
+        out_specs=specs if isinstance(out, (list, tuple)) else specs[0],
         scratch_shapes=scratch,
         cost_estimate=pl.CostEstimate(flops=flops, bytes_accessed=moved, transcendentals=0),
         compiler_params=pltpu.CompilerParams(vmem_limit_bytes=16 * 1024 * 1024),
@@ -103,12 +104,12 @@
     return jnp.concatenate(halves, axis=1)
 
 
-def first_projection_kernel(rows_ref, weights_ref, out_t_ref, fv_ref):
+def first_projection_kernel(rows_ref, weights_ref, out_t_ref, sent_ref, fv_ref, sems):
     seqs = fv_ref.shape[0]
     sources, _, pos, part = rows_ref.shape
     stretch = sources * pos
     chunk, width = out_t_ref.shape
-    rest = pltpu.roll(out_t_ref[chunk - 8 :, LANES:].astype(f32), 2, 0)
+    rest = pltpu.roll(out_t_ref[chunk - 8 :, LANES:].astype(f32), 1, 0)
     rest = jnp.concatenate([rest, jnp.zeros((8, fv_ref.shape[2] - LANES), f32)], axis=1).astype(bf16)
     both = [joined(weights_ref, chunk, k) for k in range(2)]
     for s in range(seqs):
@@ -116,6 +117,9 @@
         for k in range(2):
             fv_ref[s, :stretch, k * width : (k + 1) * width] = dot(rows, both[k], ((1,), (0,))).astype(bf16)
         fv_ref[s, stretch:, :] = rest
+        pltpu.make_async_copy(fv_ref.at[s], sent_ref.at[s], sems.at[s]).start()
+    for s in range(seqs):
+        pltpu.make_async_copy(fv_ref.at[s], sent_ref.at[s], sems.at[s]).wait()
 
 
 def put_out_rows(weights_ref, chunk, ref, base):
@@ -127,7 +131,7 @@
         ref[at : at + chunk, :LANES] = weights_ref[z, first:second, :]
         ref[at : at + whole, LANES:] = weights_ref[z, second : second + whole, :]
         ref[at + whole : at + chunk, LANES:] = jnp.zeros((8, LANES), bf16)
-        ref[at + whole : at + whole + 6, LANES:] = weights_ref[z, second + whole : second + whole + 6, :]
+        ref[at + whole : at + whole + 7, LANES:] = weights_ref[z, second + whole : second + whole + 7, :]
 
 
 def second_projection_kernel(rows_ref, weights_ref, *out_refs):
@@ -155,9 +159,9 @@
         at = base + z * chunk
         out_ref[z, :, :LANES] = ref[at : at + chunk, :LANES]
         out_ref[z, : chunk - 8, LANES:] = ref[at : at + chunk - 8, LANES:]
-        moved = pltpu.roll(piece_ref[z, rest_at:, :].astype(f32), (6 - 2 * d) % 8, 0)
+        moved = pltpu.roll(piece_ref[z, rest_at:, :].astype(f32), 7 - d, 0)
         old = ref[at + chunk - 8 : at + chunk, LANES:].astype(f32)
-        out_ref[z, chunk - 8 :, LANES:] = jnp.where(edge_row >= 6, moved, old).astype(bf16)
+        out_ref[z, chunk - 8 :, LANES:] = jnp.where(edge_row == 7, moved, old).astype(bf16)
 
 
 def gates_kernel(fv_ref, gap_ref, piece_ref, sums_ref, inkey_ref, values_ref):
@@ -186,34 +190,37 @@
     sums_ref[...] = cumulative
     inkey_ref[...] = inkey
     key_final = (inkey * jnp.exp(final - cumulative)).astype(bf16)
-    ones = jnp.ones((stretch, LANES), bf16)
     lane = lax.broadcasted_iota(jnp.int32, (8, LANES), 1)
     row = lax.broadcasted_iota(jnp.int32, (8, LANES), 0)
     rests = jnp.zeros((8, LANES), f32)
     for d in range(ny):
         source = lax.rem(lax.axis_index("y") + ny - d, ny)
         moved = fv_ref[source, stretch:, :LANES].astype(f32)
-        rests = jnp.where(row // 2 == d, pltpu.roll(moved, 2 * d, 0) if d else moved, rests)
-    rests = rests.astype(bf16)
+        rests = jnp.where(row == d, pltpu.roll(moved, d, 0) if d else moved, rests)
     per_head = KEY_DIM // mine
     for h in range(width // KEY_DIM):
         cut = slice(h * KEY_DIM, (h + 1) * KEY_DIM)
         state = dot(key_final[:, cut], values[:, cut], ((0,), (0,))).astype(bf16)
-        decay = jnp.exp(sum(dot(p[:, cut], ones, ((0,), (0,))) for p in parts))
+        decay = jnp.exp(jnp.broadcast_to(final[:, cut], (KEY_DIM, KEY_DIM)).T)
         high = decay.astype(bf16).astype(f32)
         low = (decay - high).astype(bf16).astype(f32)
         for k in range(per_head):
             at = h * per_head + k
             lower = k * mine
             piece_ref[at, :mine, :] = state[lower : lower + mine]
-            top = jnp.where(lane < 32, high[lower : lower + 8], low[lower : lower + 8])
-            bottom = jnp.where(lane < 96, high[lower + 8 : lower + 16], low[lower + 8 : lower + 16])
-            piece_ref[at, mine : mine + 8, :] = jnp.where(lane < 64, top, bottom).astype(bf16)
-            piece_ref[at, mine + 8 :, :] = rests
-
-
-def keys_kernel(sums_ref, inkey_ref, keys_ref):
-    keys_ref[...] = (inkey_ref[...] * jnp.exp(-sums_ref[...])).astype(bf16)
+            tile = None
+            for j in range(4):
+                at8 = lower + 8 * (j // 2)
+                both = jnp.where(lane % 32 < 16, high[at8 : at8 + 8], low[at8 : at8 + 8])
+                both = both if j % 2 else pltpu.roll(both, 4, 0)
+                tile = both if tile is None else jnp.where(lane < 32 * j, tile, both)
+            piece_ref[at, mine:, :] = jnp.where(row < 4, rests, tile).astype(bf16)
+
+
+def keys_kernel(sums_ref, inkey_ref, values_ref, both_ref):
+    width = inkey_ref.shape[1]
+    both_ref[:, :width] = (inkey_ref[...] * jnp.exp(-sums_ref[...])).astype(bf16)
+    both_ref[:, width:] = values_ref[...]
 
 
 def reach_kernel(sums_ref, reach_ref):
@@ -222,18 +229,18 @@
 
 def prefix_kernel(piece_ref, out_ref):
     nz, mine, _ = out_ref.shape
-    state = [jnp.zeros((8, VAL_DIM), f32) for _ in range(2)]
+    state = [jnp.zeros((4, VAL_DIM), f32) for _ in range(mine // 4)]
     for k in range(nz):
         out_ref[k] = jnp.concatenate(state, axis=0).astype(bf16)
-        packed = piece_ref[k, mine : mine + 8, :].astype(f32)
+        packed = piece_ref[k, mine:, :].astype(f32)[4:]
         added = piece_ref[k, :mine, :].astype(f32)
-        for i in range(2):
-            factor = packed[:, 64 * i : 64 * i + 1] + packed[:, 64 * i + 32 : 64 * i + 33]
-            state[i] = factor * state[i] + added[8 * i : 8 * i + 8]
+        for i in range(mine // 4):
+            factor = packed[:, 32 * i : 32 * i + 1] + packed[:, 32 * i + 16 : 32 * i + 17]
+            state[i] = factor * state[i] + added[4 * i : 4 * i + 4]
 
 
 def inside_kernel(*refs):
-    *later_refs, reach_ref, keys_ref, values_ref, piece_ref, inside_ref, out_t_ref = refs
+    *later_refs, reach_ref, both_ref, piece_ref, inside_ref, out_t_ref = refs
     stretch, width = reach_ref.shape
     query = later_refs[0][:stretch, :].astype(f32)
     for ref in later_refs[1:]:
@@ -246,9 +253,9 @@
     causal = row >= column
     for h in range(width // KEY_DIM):
         cut = slice(h * KEY_DIM, (h + 1) * KEY_DIM)
-        scores = dot(scaled[:, cut], keys_ref[:, cut], ((1,), (1,)))
+        scores = dot(scaled[:, cut], both_ref[:, cut], ((1,), (1,)))
         scores = jnp.where(causal, scores, 0.0).astype(bf16)
-        inside_ref[:, cut] = dot(scores, values_ref[:, cut], ((1,), (0,)))
+        inside_ref[:, cut] = dot(scores, both_ref[:, width + h * KEY_DIM : width + (h + 1) * KEY_DIM], ((1,), (0,)))
     for d, ref in enumerate(later_refs):
         if ref.shape[0] > stretch:
             whole_out_rows(ref, stretch, piece_ref, d, out_t_ref.at[d])
@@ -258,7 +265,8 @@
     whole_out_rows(far_ref, 0, piece_ref, far, out_ref)
 
 
-def readout_kernel(far, inside_ref, out_t_ref, far_out_ref, state_ref, gain_ref, give_ref, keep_ref):
+def readout_kernel(far, inside_ref, out_t_ref, far_out_ref, state_ref, gain_ref, *out_refs):
+    sent_ref, keep_ref, give_ref, sems = out_refs
     ny, nz, chunk, width = out_t_ref.shape
     stretch = inside_ref.shape[0]
     scaled = inside_ref[:, width:].astype(bf16)
@@ -280,8 +288,13 @@
         source = lax.rem(lax.axis_index("y") + ny - d, ny)
         columns = pl.ds(pl.multiple_of(source * part, part), part)
         mixed = dot(hidden, weight, ((1,), (1,))).astype(bf16)
-        give_ref[:, columns] = mixed[:half]
         keep_ref[:, columns] = mixed[half:]
+        give_ref[d] = mixed[:half]
+        pltpu.make_async_copy(give_ref.at[d], sent_ref.at[:, columns], sems.at[d]).start()
+    for d in range(ny):
+        source = lax.rem(lax.axis_index("y") + ny - d, ny)
+        columns = pl.ds(pl.multiple_of(source * part, part), part)
+        pltpu.make_async_copy(give_ref.at[d], sent_ref.at[:, columns], sems.at[d]).wait()
 
 
 def pair_kernel(kept_ref, given_ref, out_ref):
@@ -326,7 +339,7 @@
         lambda *refs: normalize_kernel(ny, nt, chunk, *refs),
         [
             pltpu.HBM((ny, nt, seqs * pos, part), bf16),
-            shape((8 * chunk - 2, LANES), bf16),
+            shape((8 * chunk - 1, LANES), bf16),
         ],
         1_000_000,
         *(
@@ -342,13 +355,20 @@
     far = ny // 2
 
     fv = call(
-        first_projection_kernel, shape((seqs, stretch + 8, 2 * key_width), bf16), 550_000_000, rows, weights, out_t
+        first_projection_kernel,
+        pltpu.HBM((seqs, stretch + 8, 2 * key_width), bf16),
+        550_000_000,
+        rows,
+        weights,
+        out_t,
+        scratch=[pltpu.VMEM((seqs, stretch + 8, 2 * key_width), bf16), pltpu.SemaphoreType.DMA((seqs,))],
+        copied=(0,),
     )
     fv = exchanged(fv, "y")
     pieces, sums, inkey, values = call(
         gates_kernel,
         [
-            pltpu.HBM((nz, mine + 16, VAL_DIM), bf16),
+            pltpu.HBM((nz, mine + 8, VAL_DIM), bf16),
             shape((stretch, key_width), f32),
             shape((stretch, key_width), f32),
             shape((stretch, key_width), bf16),
@@ -372,7 +392,7 @@
     later = [sent[0]] + [shifted(sent[d], d) for d in range(1, ny)]
     far_out = call(lambda *refs: far_rows_kernel(chunk, *refs), pltpu.HBM((part, key_width), bf16), 1_000_000, weights)
     far_out = shifted(far_out, far)
-    keys = call(keys_kernel, shape((stretch, key_width), bf16), 1_000_000, sums, inkey)
+    both = call(keys_kernel, shape((stretch, 2 * key_width), bf16), 1_000_000, sums, inkey, values)
     reach = call(reach_kernel, shape((stretch, key_width), f32), 1_000_000, sums)
     entering = call(prefix_kernel, shape((nz, mine, VAL_DIM), bf16), 1_000_000, pieces)
     incoming = exchanged(entering, "z").reshape(key_width, VAL_DIM)
@@ -385,8 +405,7 @@
         100_000_000,
         *later,
         reach,
-        keys,
-        values,
+        both,
         pieces,
     )
     far_out = call(
@@ -401,6 +420,8 @@
         far_out,
         incoming,
         head_gain.reshape(1, key_width),
+        scratch=[pltpu.VMEM((ny, stretch // 2, part), bf16), pltpu.SemaphoreType.DMA((ny,))],
+        copied=(0,),
     )
     given = lax.ppermute(give, "c", [(0, 1), (1, 0)])
     mixed = call(pair_kernel, shape((stretch // 2, width), bf16), 1_000_000, kept, given)

time: 140 us -> 141 us (level)
  no operation moved by 1% of the time
where the time goes in v1:
time: 141 us; the launch traced here: 140 us
  blocking collectives  65.6 us (47%)
  starting transfers between devices  53.1 us (38%)
  Pallas kernels  12.3 us (9%)
  waiting for transfers between devices  7.16 us (5%)
  local copies, waits for them, and re-layouts  1.77 us (1%)
    all_gather x1, blocking collectives, block(): weights = lax.all_gather(packed, 'z', axis=0)  33.6 us
    all_to_all x2, blocking collectives, exchanged(): return lax.all_to_all(value, axis, 0, 0, tiled=True)  32 us
    all_to_all x3, starting transfers between devices, exchanged(): return lax.all_to_all(value, axis, 0, 0, tiled=True)  27.9 us
    ppermute x4, starting transfers between devices, shifted(): return lax.ppermute(value, 'y', [(i, (i + d) % ny) for i in range(ny)])  13.4 us
    pallas_call x13, Pallas kernels, call(): pl.pallas_call(kernel, out_shape=out, in_specs=[pl.BlockSpec(memory_space...  12.3 us
    ppermute x1, starting transfers between devices, block(): given = lax.ppermute(give, 'c', [(0, 1), (1, 0)])  11.8 us
    all_to_all x3, waiting for transfers between devices, exchanged(): return lax.all_to_all(value, axis, 0, 0, tiled=True)  3.05 us
  transfers between devices with their start and end apart: 8, of which 4 were waited for; matrix products, arithmetic and copies ran while one was open for 0% of the time, Pallas kernels for 3%

profile of v1, /device:TPU:1, one launch (start us, length us, event | category | flops | bytes accessed | tf_op | source)
XLA Modules:
  0.0 140.1 jit_solution(3900542063260476292)
XLA Ops:
  0.0 2.4 %shard_map.82 = (bf16[4,8,32,512]{3,2,1,0:T(8,128)(2,1)}, bf16[255,128]{1,0:T(8,128)(2,1)S(1)}) custom-call(bf16[8,4,2048]{2,1,0:T(4,128)(2,1)} %refs_0_.1, f32[1,2048]{1,0:T(1,128)} %bitcast.17, bf16[32,256]{1,0:T(8,128)(2,1)} %refs_2_.1, bf16[32,256]{1,0:T(8,128)(2,1)} %refs_3_.1, bf16[32,256]{1,0:T(8,128)(2,1)} %refs_4_.1, bf16[32,256]{1,0:T(8,128)(2,1)} %bitcast.11), custom_call_target="tpu_custom_call" | custom-call | flops 1000000 | bytes 1318656 | tf_op jit(solution)/shard_map/pallas_call | solution.py:30
  2.4 10.4 %all-to-all-start = ((bf16[32,4,8,512]{3,2,1,0:T(8,128)(2,1)}), bf16[32,4,8,512]{3,2,1,0:T(8,128)(2,1)S(1)}, u32[]{:S(2)}, u32[]{:S(2)}) async-start(bf16[32,4,8,512]{3,2,1,0:T(8,128)(2,1)} %bitcast.16), calls=%async_computation | async-start | bytes 2097152 | tf_op jit(solution)/shard_map/all_to_all | solution.py:23
  12.8 0.0 copy-start.5
  12.8 33.6 %all-gather.1.weights_ref.refs_0_ = bf16[16,255,128]{2,1,0:T(8,128)(2,1)S(1)} all-gather(bf16[1,255,128]{2,1,0:T(8,128)(2,1)S(1)} %bitcast.13), channel_id=2, replica_groups=mesh['z'=16,'y'=4,'x'=4,'c'=2] {'z'}, dimensions={0}, use_global_device_ids=true | all-gather | bytes 1109760 | tf_op jit(solution)/shard_map/all_gather | solution.py:353
  46.5 0.0 all-to-all-done.rows_ref
  46.5 0.0 copy-done.5
  46.5 1.5 %shard_map.84 = bf16[4,264,512]{2,1,0:T(8,128)(2,1)} custom-call(bf16[32,4,8,512]{3,2,1,0:T(8,128)(2,1)S(1)} %all-to-all-done.rows_ref, bf16[16,255,128]{2,1,0:T(8,128)(2,1)S(1)} %all-gather.1.weights_ref.refs_0_, bf16[32,256]{1,0:T(8,128)(2,1)S(1)} %bitcast.12), custom_call_target="tpu_custom_call" | custom-call | flops 550000000 | bytes 3190784 | tf_op jit(solution)/shard_map/pallas_call | solution.py:30
  47.9 0.0 copy-start.7
  48.0 14.3 %all_to_all.25.fv_ref = bf16[4,264,512]{2,1,0:T(8,128)(2,1)S(1)} all-to-all(bf16[4,264,512]{2,1,0:T(8,128)(2,1)} %shard_map.84), channel_id=1, replica_groups=mesh['z'=16,'y'=4,'x'=4,'c'=2] {'y'}, dimensions={0} | all-to-all | bytes 2162688 | tf_op jit(solution)/shard_map/all_to_all | solution.py:23
  62.3 0.0 copy-done.7
  62.3 1.4 %shard_map.85 = (bf16[16,24,128]{2,1,0:T(8,128)(2,1)}, f32[256,256]{1,0:T(8,128)S(1)}, f32[256,256]{1,0:T(8,128)S(1)}, bf16[256,256]{1,0:T(8,128)(2,1)S(1)}) custom-call(bf16[4,264,512]{2,1,0:T(8,128)(2,1)S(1)} %all_to_all.25.fv_ref, f32[1,256]{1,0:T(1,128)S(1)} %bitcast.15), custom_call_target="tpu_custom_call" | custom-call | flops 100000000 | bytes 1836032 | tf_op jit(solution)/shard_map/pallas_call | solution.py:30
  63.7 0.0 copy-start.3
  63.7 7.0 %all-to-all-start.2 = ((bf16[16,24,128]{2,1,0:T(8,128)(2,1)}), bf16[16,24,128]{2,1,0:T(8,128)(2,1)S(1)}, u32[]{:S(2)}, u32[]{:S(2)}) async-start(bf16[16,24,128]{2,1,0:T(8,128)(2,1)} %get-tuple-element.28), calls=%async_computation.2 | async-start | bytes 196608 | tf_op jit(solution)/shard_map/all_to_all | solution.py:23
  70.7 1.5 %shard_map.83 = (bf16[768,256]{1,0:T(8,128)(2,1)}, bf16[768,256]{1,0:T(8,128)(2,1)}, bf16[256,256]{1,0:T(8,128)(2,1)}, bf16[768,256]{1,0:T(8,128)(2,1)}) custom-call(bf16[32,4,8,512]{3,2,1,0:T(8,128)(2,1)S(1)} %all-to-all-done.rows_ref, bf16[16,255,128]{2,1,0:T(8,128)(2,1)S(1)} %all-gather.1.weights_ref.refs_0_), custom_call_target="tpu_custom_call" | custom-call | flops 280000000 | bytes 3403776 | tf_op jit(solution)/shard_map/pallas_call | solution.py:30
  72.2 0.0 copy-done.3
  72.2 0.0 copy-start.4
  72.2 2.3 %collective-permute-start = (bf16[768,256]{1,0:T(8,128)(2,1)}, bf16[768,256]{1,0:T(8,128)(2,1)S(1)}, u32[]{:S(2)}, u32[]{:S(2)}) collective-permute-start(bf16[768,256]{1,0:T(8,128)(2,1)} %get-tuple-element.22), channel_id=1, source_target_pairs={{0,8},{8,16},{16,24},{24,0},{1,9},{9,17},{17,25},{25,1},{2,10},{10... | collective-permute-start | bytes 1179656 | tf_op jit(solution)/shard_map/ppermute | solution.py:390
  74.5 4.3 %collective-permute-start.2 = (bf16[768,256]{1,0:T(8,128)(2,1)}, bf16[768,256]{1,0:T(8,128)(2,1)S(1)}, u32[]{:S(2)}, u32[]{:S(2)}) collective-permute-start(bf16[768,256]{1,0:T(8,128)(2,1)} %get-tuple-element.24), channel_id=1, source_target_pairs={{0,24},{8,0},{16,8},{24,16},{1,25},{9,1},{17,9},{25,17},{2,26},{10... | collective-permute-start | bytes 1179656 | tf_op jit(solution)/shard_map/ppermute | solution.py:390
  78.8 0.8 shard_map.89
  79.6 1.9 %collective-permute-start.3 = (bf16[512,256]{1,0:T(8,128)(2,1)}, bf16[512,256]{1,0:T(8,128)(2,1)S(1)}, u32[]{:S(2)}, u32[]{:S(2)}) collective-permute-start(bf16[512,256]{1,0:T(8,128)(2,1)} %shard_map.89), channel_id=1, source_target_pairs={{0,16},{8,24},{16,0},{24,8},{1,17},{9,25},{17,1},{25,9},{2,18},{10... | collective-permute-start | bytes 786440 | tf_op jit(solution)/shard_map/ppermute | solution.py:390
  81.5 1.1 all-to-all-done.2.refs_6_.refs_1_.piece_ref
  82.6 0.9 shard_map.91
  83.5 0.0 copy-start
  83.5 10.5 %all-to-all-start.3 = ((bf16[16,16,128]{2,1,0:T(8,128)(2,1)}), bf16[16,16,128]{2,1,0:T(8,128)(2,1)}, u32[]{:S(2)}, u32[]{:S(2)}) async-start(bf16[16,16,128]{2,1,0:T(8,128)(2,1)} %shard_map.91), calls=%async_computation.3 | async-start | bytes 131072 | tf_op jit(solution)/shard_map/all_to_all | solution.py:23
  94.0 4.9 %collective-permute-start.1 = (bf16[256,256]{1,0:T(8,128)(2,1)}, bf16[256,256]{1,0:T(8,128)(2,1)S(1)}, u32[]{:S(2)}, u32[]{:S(2)}) collective-permute-start(bf16[256,256]{1,0:T(8,128)(2,1)} %get-tuple-element.23), channel_id=1, source_target_pairs={{0,16},{8,24},{16,0},{24,8},{1,17},{9,25},{17,1},{25,9},{2,18},{10... | collective-permute-start | bytes 393224 | tf_op jit(solution)/shard_map/ppermute | solution.py:390
  98.9 0.0 copy-done.4
  98.9 0.1 shard_map.87.refs_5_
  99.0 0.0 collective-permute-done.3.refs_0_
  99.0 0.0 copy-start.6
  99.1 2.4 %collective-permute-done.1.refs_2_ = bf16[256,256]{1,0:T(8,128)(2,1)S(1)} collective-permute-done((bf16[256,256]{1,0:T(8,128)(2,1)}, bf16[256,256]{1,0:T(8,128)(2,1)S(1)}, u32[]{:S(2)}, u32[]{:S(2)}) %collective-permute-start.1) | collective-permute-done | bytes 131104 | tf_op jit(solution)/shard_map/ppermute | solution.py:390
  101.4 0.0 collective-permute-done.refs_1_
  101.4 0.0 collective-permute-done.2.refs_3_
  101.4 0.0 copy-start.1
  101.4 0.7 copy-done.1
  102.2 0.0 copy-done
  102.2 0.0 copy-start.2
  102.2 1.0 copy-done.2
  103.2 0.5 shard_map.88
  103.7 1.9 %all-to-all-done.3 = bf16[16,16,128]{2,1,0:T(8,128)(2,1)} async-done(((bf16[16,16,128]{2,1,0:T(8,128)(2,1)}), bf16[16,16,128]{2,1,0:T(8,128)(2,1)}, u32[]{:S(2)}, u32[]{:S(2)}) %all-to-all-start.3) | async-done | bytes 65568 | tf_op jit(solution)/shard_map/all_to_all | solution.py:23
  105.6 0.0 copy-done.6
  105.6 2.2 %shard_map.92 = (bf16[128,2048]{1,0:T(8,128)(2,1)}, bf16[128,2048]{1,0:T(8,128)(2,1)S(1)}) custom-call(f32[256,512]{1,0:T(8,128)S(1)} %get-tuple-element.29.refs_0_, bf16[4,16,32,256]{3,2,1,0:T(8,128)(2,1)S(1)} %get-tuple-element.30.refs_1_, bf16[16,32,256]{2,1,0:T(8,128)(2,1)S(1)} %shard_map.90.refs_2_, bf16[256,128]{1,0:T(8,128)(2,1)} %bitcast.5.refs_3_, ...), custom_call_target="tpu_custom_call" | custom-call | flops 300000000 | bytes 2950144 | tf_op jit(solution)/shard_map/pallas_call | solution.py:30
  107.8 11.8 %collective-permute-start.4 = (bf16[128,2048]{1,0:T(8,128)(2,1)}, bf16[128,2048]{1,0:T(8,128)(2,1)S(1)}, u32[]{:S(2)}, u32[]{:S(2)}) collective-permute-start(bf16[128,2048]{1,0:T(8,128)(2,1)} %get-tuple-element.32), channel_id=1, source_target_pairs={{0,1},{1,0},{2,3},{3,2},{4,5},{5,4},{6,7},{7,6},{8,9},{9,8},{10,11... | collective-permute-start | bytes 1572872 | tf_op jit(solution)/shard_map/ppermute | solution.py:426
  119.6 1.7 %collective-permute-done.4.given_ref = bf16[128,2048]{1,0:T(8,128)(2,1)S(1)} collective-permute-done((bf16[128,2048]{1,0:T(8,128)(2,1)}, bf16[128,2048]{1,0:T(8,128)(2,1)S(1)}, u32[]{:S(2)}, u32[]{:S(2)}) %collective-permute-start.4) | collective-permute-done | bytes 524320 | tf_op jit(solution)/shard_map/ppermute | solution.py:426
  121.4 0.1 shard_map.93
  121.5 17.7 %all_to_all.26 = bf16[16,8,2048]{2,1,0:T(8,128)(2,1)S(1)} all-to-all(bf16[16,8,2048]{2,1,0:T(8,128)(2,1)S(1)} %bitcast.9), channel_id=1, replica_groups=mesh['z'=16,'y'=4,'x'=4,'c'=2] {'y','x'}, dimensions={0} | all-to-all | bytes 1048576 | tf_op jit(solution)/shard_map/all_to_all | solution.py:23
  139.1 1.0 shard_map.94
  (2 shorter events, 0.1 us)
Async XLA Ops:
  2.4 44.1 %all-to-all-start = ((bf16[32,4,8,512]{3,2,1,0:T(8,128)(2,1)}), bf16[32,4,8,512]{3,2,1,0:T(8,128)(2,1)S(1)}, u32[]{:S(2)}, u32[]{:S(2)}) async-start(bf16[32,4,8,512]{3,2,1,0:T(8,128)(2,1)} %bitcast.16), calls=%async_computation | async-start | bytes 2097152 | tf_op jit(solution)/shard_map/all_to_all | solution.py:23
  12.8 33.7 %copy-start.5 = (bf16[256,32]{0,1:T(8,128)(2,1)S(1)}, bf16[256,32]{0,1:T(8,128)(2,1)}, u32[]{:S(2)}) copy-start(bf16[256,32]{0,1:T(8,128)(2,1)} %param.15) | copy-start | bytes 49156
  47.9 14.4 %copy-start.7 = (f32[256]{0:T(256)S(1)}, f32[256]{0:T(256)}, u32[]{:S(2)}) copy-start(f32[256]{0:T(256)} %param.13) | copy-start | bytes 3076
  63.7 8.5 %copy-start.3 = (bf16[256,256]{1,0:T(8,128)(2,1)}, bf16[256,256]{1,0:T(8,128)(2,1)S(1)}, u32[]{:S(2)}) copy-start(bf16[256,256]{1,0:T(8,128)(2,1)S(1)} %get-tuple-element.27.values_ref) | copy-start | bytes 393220
  63.7 18.9 %all-to-all-start.2 = ((bf16[16,24,128]{2,1,0:T(8,128)(2,1)}), bf16[16,24,128]{2,1,0:T(8,128)(2,1)S(1)}, u32[]{:S(2)}, u32[]{:S(2)}) async-start(bf16[16,24,128]{2,1,0:T(8,128)(2,1)} %get-tuple-element.28), calls=%async_computation.2 | async-start | bytes 196608 | tf_op jit(solution)/shard_map/all_to_all | solution.py:23
  72.2 26.8 %copy-start.4 = (bf16[256,256]{1,0:T(8,128)(2,1)S(1)}, bf16[256,256]{1,0:T(8,128)(2,1)}, u32[]{:S(2)}) copy-start(bf16[256,256]{1,0:T(8,128)(2,1)} %copy-done.3) | copy-start | bytes 393220
  72.2 29.3 %collective-permute-start = (bf16[768,256]{1,0:T(8,128)(2,1)}, bf16[768,256]{1,0:T(8,128)(2,1)S(1)}, u32[]{:S(2)}, u32[]{:S(2)}) collective-permute-start(bf16[768,256]{1,0:T(8,128)(2,1)} %get-tuple-element.22), channel_id=1, source_target_pairs={{0,8},{8,16},{16,24},{24,0},{1,9},{9,17},{17,25},{25,1},{2,10},{10... | collective-permute-start | bytes 1179656 | tf_op jit(solution)/shard_map/ppermute | solution.py:390
  74.5 26.9 %collective-permute-start.2 = (bf16[768,256]{1,0:T(8,128)(2,1)}, bf16[768,256]{1,0:T(8,128)(2,1)S(1)}, u32[]{:S(2)}, u32[]{:S(2)}) collective-permute-start(bf16[768,256]{1,0:T(8,128)(2,1)} %get-tuple-element.24), channel_id=1, source_target_pairs={{0,24},{8,0},{16,8},{24,16},{1,25},{9,1},{17,9},{25,17},{2,26},{10... | collective-permute-start | bytes 1179656 | tf_op jit(solution)/shard_map/ppermute | solution.py:390
  79.6 19.4 %collective-permute-start.3 = (bf16[512,256]{1,0:T(8,128)(2,1)}, bf16[512,256]{1,0:T(8,128)(2,1)S(1)}, u32[]{:S(2)}, u32[]{:S(2)}) collective-permute-start(bf16[512,256]{1,0:T(8,128)(2,1)} %shard_map.89), channel_id=1, source_target_pairs={{0,16},{8,24},{16,0},{24,8},{1,17},{9,25},{17,1},{25,9},{2,18},{10... | collective-permute-start | bytes 786440 | tf_op jit(solution)/shard_map/ppermute | solution.py:390
  83.5 18.7 %copy-start = (bf16[768,256]{1,0:T(8,128)(2,1)S(1)}, bf16[768,256]{1,0:T(8,128)(2,1)}, u32[]{:S(2)}) copy-start(bf16[768,256]{1,0:T(8,128)(2,1)} %get-tuple-element.21.refs_0_) | copy-start | bytes 1179652
  83.5 22.1 %all-to-all-start.3 = ((bf16[16,16,128]{2,1,0:T(8,128)(2,1)}), bf16[16,16,128]{2,1,0:T(8,128)(2,1)}, u32[]{:S(2)}, u32[]{:S(2)}) async-start(bf16[16,16,128]{2,1,0:T(8,128)(2,1)} %shard_map.91), calls=%async_computation.3 | async-start | bytes 131072 | tf_op jit(solution)/shard_map/all_to_all | solution.py:23
  94.0 7.4 %collective-permute-start.1 = (bf16[256,256]{1,0:T(8,128)(2,1)}, bf16[256,256]{1,0:T(8,128)(2,1)S(1)}, u32[]{:S(2)}, u32[]{:S(2)}) collective-permute-start(bf16[256,256]{1,0:T(8,128)(2,1)} %get-tuple-element.23), channel_id=1, source_target_pairs={{0,16},{8,24},{16,0},{24,8},{1,17},{9,25},{17,1},{25,9},{2,18},{10... | collective-permute-start | bytes 393224 | tf_op jit(solution)/shard_map/ppermute | solution.py:390
  99.0 6.6 %copy-start.6 = (f32[256]{0:T(256)S(1)}, f32[256]{0:T(256)}, u32[]{:S(2)}) copy-start(f32[256]{0:T(256)} %param.14) | copy-start | bytes 3076
  101.4 0.7 copy-start.1
  102.2 1.0 copy-start.2
  107.8 13.5 %collective-permute-start.4 = (bf16[128,2048]{1,0:T(8,128)(2,1)}, bf16[128,2048]{1,0:T(8,128)(2,1)S(1)}, u32[]{:S(2)}, u32[]{:S(2)}) collective-permute-start(bf16[128,2048]{1,0:T(8,128)(2,1)} %get-tuple-element.32), channel_id=1, source_target_pairs={{0,1},{1,0},{2,3},{3,2},{4,5},{5,4},{6,7},{7,6},{8,9},{9,8},{10,11... | collective-permute-start | bytes 1572872 | tf_op jit(solution)/shard_map/ppermute | solution.py:426

commit v2 on v1

--- a/solution.py
+++ b/solution.py
@@ -117,7 +117,9 @@
         for k in range(2):
             fv_ref[s, :stretch, k * width : (k + 1) * width] = dot(rows, both[k], ((1,), (0,))).astype(bf16)
         fv_ref[s, stretch:, :] = rest
-        pltpu.make_async_copy(fv_ref.at[s], sent_ref.at[s], sems.at[s]).start()
+        if s > 0:
+            pltpu.make_async_copy(fv_ref.at[s - 1], sent_ref.at[s - 1], sems.at[s - 1]).start()
+    pltpu.make_async_copy(fv_ref.at[seqs - 1], sent_ref.at[seqs - 1], sems.at[seqs - 1]).start()
     for s in range(seqs):
         pltpu.make_async_copy(fv_ref.at[s], sent_ref.at[s], sems.at[s]).wait()
 
@@ -283,18 +285,24 @@
     hidden = jnp.concatenate([jnp.where(at_first, second, first), jnp.where(at_first, first, second)], axis=0)
     hidden = hidden.astype(bf16)
     part = nz * chunk
+
+    def columns(d):
+        source = lax.rem(lax.axis_index("y") + ny - d, ny)
+        return pl.ds(pl.multiple_of(source * part, part), part)
+
+    def copy(d):
+        return pltpu.make_async_copy(give_ref.at[d], sent_ref.at[:, columns(d)], sems.at[d])
+
     for d in range(ny):
         weight = (far_out_ref[...] if d == far else out_t_ref[d]).reshape(part, width)
-        source = lax.rem(lax.axis_index("y") + ny - d, ny)
-        columns = pl.ds(pl.multiple_of(source * part, part), part)
         mixed = dot(hidden, weight, ((1,), (1,))).astype(bf16)
-        keep_ref[:, columns] = mixed[half:]
+        keep_ref[:, columns(d)] = mixed[half:]
         give_ref[d] = mixed[:half]
-        pltpu.make_async_copy(give_ref.at[d], sent_ref.at[:, columns], sems.at[d]).start()
+        if d > 0:
+            copy(d - 1).start()
+    copy(ny - 1).start()
     for d in range(ny):
-        source = lax.rem(lax.axis_index("y") + ny - d, ny)
-        columns = pl.ds(pl.multiple_of(source * part, part), part)
-        pltpu.make_async_copy(give_ref.at[d], sent_ref.at[:, columns], sems.at[d]).wait()
+        copy(d).wait()
 
 
 def pair_kernel(kept_ref, given_ref, out_ref):

time: 141 us -> 141 us (level)
  no operation moved by 1% of the time
where the time goes in v2:
time: 141 us; the launch traced here: 140 us
  blocking collectives  65.6 us (47%)
  starting transfers between devices  53.1 us (38%)
  Pallas kernels  12.4 us (9%)
  waiting for transfers between devices  7.16 us (5%)
  local copies, waits for them, and re-layouts  1.77 us (1%)
    all_gather x1, blocking collectives, block(): weights = lax.all_gather(packed, 'z', axis=0)  33.6 us
    all_to_all x2, blocking collectives, exchanged(): return lax.all_to_all(value, axis, 0, 0, tiled=True)  32 us
    all_to_all x3, starting transfers between devices, exchanged(): return lax.all_to_all(value, axis, 0, 0, tiled=True)  27.9 us
    ppermute x4, starting transfers between devices, shifted(): return lax.ppermute(value, 'y', [(i, (i + d) % ny) for i in range(ny)])  13.4 us
    pallas_call x13, Pallas kernels, call(): pl.pallas_call(kernel, out_shape=out, in_specs=[pl.BlockSpec(memory_space...  12.4 us
    ppermute x1, starting transfers between devices, block(): given = lax.ppermute(give, 'c', [(0, 1), (1, 0)])  11.8 us
    all_to_all x3, waiting for transfers between devices, exchanged(): return lax.all_to_all(value, axis, 0, 0, tiled=True)  3.05 us
  transfers between devices with their start and end apart: 8, of which 4 were waited for; matrix products, arithmetic and copies ran while one was open for 0% of the time, Pallas kernels for 3%

profile of v2, /device:TPU:1, one launch (start us, length us, event | category | flops | bytes accessed | tf_op | source)
XLA Modules:
  0.0 140.3 jit_solution(7883322864700567162)
XLA Ops:
  0.0 2.4 %shard_map.82 = (bf16[4,8,32,512]{3,2,1,0:T(8,128)(2,1)}, bf16[255,128]{1,0:T(8,128)(2,1)S(1)}) custom-call(bf16[8,4,2048]{2,1,0:T(4,128)(2,1)} %refs_0_.1, f32[1,2048]{1,0:T(1,128)} %bitcast.17, bf16[32,256]{1,0:T(8,128)(2,1)} %refs_2_.1, bf16[32,256]{1,0:T(8,128)(2,1)} %refs_3_.1, bf16[32,256]{1,0:T(8,128)(2,1)} %refs_4_.1, bf16[32,256]{1,0:T(8,128)(2,1)} %bitcast.11), custom_call_target="tpu_custom_call" | custom-call | flops 1000000 | bytes 1318656 | tf_op jit(solution)/shard_map/pallas_call | solution.py:30
  2.4 10.4 %all-to-all-start = ((bf16[32,4,8,512]{3,2,1,0:T(8,128)(2,1)}), bf16[32,4,8,512]{3,2,1,0:T(8,128)(2,1)S(1)}, u32[]{:S(2)}, u32[]{:S(2)}) async-start(bf16[32,4,8,512]{3,2,1,0:T(8,128)(2,1)} %bitcast.16), calls=%async_computation | async-start | bytes 2097152 | tf_op jit(solution)/shard_map/all_to_all | solution.py:23
  12.8 0.0 copy-start.5
  12.8 33.6 %all-gather.1.weights_ref.refs_0_ = bf16[16,255,128]{2,1,0:T(8,128)(2,1)S(1)} all-gather(bf16[1,255,128]{2,1,0:T(8,128)(2,1)S(1)} %bitcast.13), channel_id=2, replica_groups=mesh['z'=16,'y'=4,'x'=4,'c'=2] {'z'}, dimensions={0}, use_global_device_ids=true | all-gather | bytes 1109760 | tf_op jit(solution)/shard_map/all_gather | solution.py:361
  46.5 0.0 all-to-all-done.rows_ref
  46.5 0.0 copy-done.5
  46.5 1.6 %shard_map.84 = bf16[4,264,512]{2,1,0:T(8,128)(2,1)} custom-call(bf16[32,4,8,512]{3,2,1,0:T(8,128)(2,1)S(1)} %all-to-all-done.rows_ref, bf16[16,255,128]{2,1,0:T(8,128)(2,1)S(1)} %all-gather.1.weights_ref.refs_0_, bf16[32,256]{1,0:T(8,128)(2,1)S(1)} %bitcast.12), custom_call_target="tpu_custom_call" | custom-call | flops 550000000 | bytes 3190784 | tf_op jit(solution)/shard_map/pallas_call | solution.py:30
  48.0 0.0 copy-start.7
  48.1 14.3 %all_to_all.25.fv_ref = bf16[4,264,512]{2,1,0:T(8,128)(2,1)S(1)} all-to-all(bf16[4,264,512]{2,1,0:T(8,128)(2,1)} %shard_map.84), channel_id=1, replica_groups=mesh['z'=16,'y'=4,'x'=4,'c'=2] {'y'}, dimensions={0} | all-to-all | bytes 2162688 | tf_op jit(solution)/shard_map/all_to_all | solution.py:23
  62.4 0.0 copy-done.7
  62.4 1.4 shard_map.85
  63.8 0.0 copy-start.3
  63.8 7.0 %all-to-all-start.2 = ((bf16[16,24,128]{2,1,0:T(8,128)(2,1)}), bf16[16,24,128]{2,1,0:T(8,128)(2,1)S(1)}, u32[]{:S(2)}, u32[]{:S(2)}) async-start(bf16[16,24,128]{2,1,0:T(8,128)(2,1)} %get-tuple-element.28), calls=%async_computation.2 | async-start | bytes 196608 | tf_op jit(solution)/shard_map/all_to_all | solution.py:23
  70.8 1.5 %shard_map.83 = (bf16[768,256]{1,0:T(8,128)(2,1)}, bf16[768,256]{1,0:T(8,128)(2,1)}, bf16[256,256]{1,0:T(8,128)(2,1)}, bf16[768,256]{1,0:T(8,128)(2,1)}) custom-call(bf16[32,4,8,512]{3,2,1,0:T(8,128)(2,1)S(1)} %all-to-all-done.rows_ref, bf16[16,255,128]{2,1,0:T(8,128)(2,1)S(1)} %all-gather.1.weights_ref.refs_0_), custom_call_target="tpu_custom_call" | custom-call | flops 280000000 | bytes 3403776 | tf_op jit(solution)/shard_map/pallas_call | solution.py:30
  72.3 0.0 copy-done.3
  72.3 0.0 copy-start.4
  72.3 2.3 %collective-permute-start = (bf16[768,256]{1,0:T(8,128)(2,1)}, bf16[768,256]{1,0:T(8,128)(2,1)S(1)}, u32[]{:S(2)}, u32[]{:S(2)}) collective-permute-start(bf16[768,256]{1,0:T(8,128)(2,1)} %get-tuple-element.22), channel_id=1, source_target_pairs={{0,8},{8,16},{16,24},{24,0},{1,9},{9,17},{17,25},{25,1},{2,10},{10... | collective-permute-start | bytes 1179656 | tf_op jit(solution)/shard_map/ppermute | solution.py:398
  74.6 4.3 %collective-permute-start.2 = (bf16[768,256]{1,0:T(8,128)(2,1)}, bf16[768,256]{1,0:T(8,128)(2,1)S(1)}, u32[]{:S(2)}, u32[]{:S(2)}) collective-permute-start(bf16[768,256]{1,0:T(8,128)(2,1)} %get-tuple-element.24), channel_id=1, source_target_pairs={{0,24},{8,0},{16,8},{24,16},{1,25},{9,1},{17,9},{25,17},{2,26},{10... | collective-permute-start | bytes 1179656 | tf_op jit(solution)/shard_map/ppermute | solution.py:398
  78.9 0.8 shard_map.89
  79.7 1.9 %collective-permute-start.3 = (bf16[512,256]{1,0:T(8,128)(2,1)}, bf16[512,256]{1,0:T(8,128)(2,1)S(1)}, u32[]{:S(2)}, u32[]{:S(2)}) collective-permute-start(bf16[512,256]{1,0:T(8,128)(2,1)} %shard_map.89), channel_id=1, source_target_pairs={{0,16},{8,24},{16,0},{24,8},{1,17},{9,25},{17,1},{25,9},{2,18},{10... | collective-permute-start | bytes 786440 | tf_op jit(solution)/shard_map/ppermute | solution.py:398
  81.6 1.1 all-to-all-done.2.refs_6_.refs_1_.piece_ref
  82.7 0.9 shard_map.91
  83.6 0.0 copy-start
  83.6 10.5 %all-to-all-start.3 = ((bf16[16,16,128]{2,1,0:T(8,128)(2,1)}), bf16[16,16,128]{2,1,0:T(8,128)(2,1)}, u32[]{:S(2)}, u32[]{:S(2)}) async-start(bf16[16,16,128]{2,1,0:T(8,128)(2,1)} %shard_map.91), calls=%async_computation.3 | async-start | bytes 131072 | tf_op jit(solution)/shard_map/all_to_all | solution.py:23
  94.1 4.9 %collective-permute-start.1 = (bf16[256,256]{1,0:T(8,128)(2,1)}, bf16[256,256]{1,0:T(8,128)(2,1)S(1)}, u32[]{:S(2)}, u32[]{:S(2)}) collective-permute-start(bf16[256,256]{1,0:T(8,128)(2,1)} %get-tuple-element.23), channel_id=1, source_target_pairs={{0,16},{8,24},{16,0},{24,8},{1,17},{9,25},{17,1},{25,9},{2,18},{10... | collective-permute-start | bytes 393224 | tf_op jit(solution)/shard_map/ppermute | solution.py:398
  99.0 0.0 copy-done.4
  99.0 0.1 shard_map.87.refs_5_
  99.1 0.0 collective-permute-done.3.refs_0_
  99.1 0.0 copy-start.6
  99.2 2.4 %collective-permute-done.1.refs_2_ = bf16[256,256]{1,0:T(8,128)(2,1)S(1)} collective-permute-done((bf16[256,256]{1,0:T(8,128)(2,1)}, bf16[256,256]{1,0:T(8,128)(2,1)S(1)}, u32[]{:S(2)}, u32[]{:S(2)}) %collective-permute-start.1) | collective-permute-done | bytes 131104 | tf_op jit(solution)/shard_map/ppermute | solution.py:398
  101.5 0.0 collective-permute-done.refs_1_
  101.5 0.0 collective-permute-done.2.refs_3_
  101.5 0.0 copy-start.1
  101.5 0.7 copy-done.1
  102.3 0.0 copy-done
  102.3 0.0 copy-start.2
  102.3 1.0 copy-done.2
  103.3 0.5 shard_map.88
  103.8 1.9 %all-to-all-done.3 = bf16[16,16,128]{2,1,0:T(8,128)(2,1)} async-done(((bf16[16,16,128]{2,1,0:T(8,128)(2,1)}), bf16[16,16,128]{2,1,0:T(8,128)(2,1)}, u32[]{:S(2)}, u32[]{:S(2)}) %all-to-all-start.3) | async-done | bytes 65568 | tf_op jit(solution)/shard_map/all_to_all | solution.py:23
  105.7 0.0 copy-done.6
  105.7 2.2 %shard_map.92 = (bf16[128,2048]{1,0:T(8,128)(2,1)}, bf16[128,2048]{1,0:T(8,128)(2,1)S(1)}) custom-call(f32[256,512]{1,0:T(8,128)S(1)} %get-tuple-element.29.refs_0_, bf16[4,16,32,256]{3,2,1,0:T(8,128)(2,1)S(1)} %get-tuple-element.30.refs_1_, bf16[16,32,256]{2,1,0:T(8,128)(2,1)S(1)} %shard_map.90.refs_2_, bf16[256,128]{1,0:T(8,128)(2,1)} %bitcast.5.refs_3_, ...), custom_call_target="tpu_custom_call" | custom-call | flops 300000000 | bytes 2950144 | tf_op jit(solution)/shard_map/pallas_call | solution.py:30
  108.0 11.8 %collective-permute-start.4 = (bf16[128,2048]{1,0:T(8,128)(2,1)}, bf16[128,2048]{1,0:T(8,128)(2,1)S(1)}, u32[]{:S(2)}, u32[]{:S(2)}) collective-permute-start(bf16[128,2048]{1,0:T(8,128)(2,1)} %get-tuple-element.32), channel_id=1, source_target_pairs={{0,1},{1,0},{2,3},{3,2},{4,5},{5,4},{6,7},{7,6},{8,9},{9,8},{10,11... | collective-permute-start | bytes 1572872 | tf_op jit(solution)/shard_map/ppermute | solution.py:434
  119.8 1.7 %collective-permute-done.4.given_ref = bf16[128,2048]{1,0:T(8,128)(2,1)S(1)} collective-permute-done((bf16[128,2048]{1,0:T(8,128)(2,1)}, bf16[128,2048]{1,0:T(8,128)(2,1)S(1)}, u32[]{:S(2)}, u32[]{:S(2)}) %collective-permute-start.4) | collective-permute-done | bytes 524320 | tf_op jit(solution)/shard_map/ppermute | solution.py:434
  121.5 0.1 shard_map.93
  121.6 17.7 %all_to_all.26 = bf16[16,8,2048]{2,1,0:T(8,128)(2,1)S(1)} all-to-all(bf16[16,8,2048]{2,1,0:T(8,128)(2,1)S(1)} %bitcast.9), channel_id=1, replica_groups=mesh['z'=16,'y'=4,'x'=4,'c'=2] {'y','x'}, dimensions={0} | all-to-all | bytes 1048576 | tf_op jit(solution)/shard_map/all_to_all | solution.py:23
  139.3 1.0 shard_map.94
  (2 shorter events, 0.1 us)
Async XLA Ops:
  2.4 44.1 %all-to-all-start = ((bf16[32,4,8,512]{3,2,1,0:T(8,128)(2,1)}), bf16[32,4,8,512]{3,2,1,0:T(8,128)(2,1)S(1)}, u32[]{:S(2)}, u32[]{:S(2)}) async-start(bf16[32,4,8,512]{3,2,1,0:T(8,128)(2,1)} %bitcast.16), calls=%async_computation | async-start | bytes 2097152 | tf_op jit(solution)/shard_map/all_to_all | solution.py:23
  12.8 33.7 %copy-start.5 = (bf16[256,32]{0,1:T(8,128)(2,1)S(1)}, bf16[256,32]{0,1:T(8,128)(2,1)}, u32[]{:S(2)}) copy-start(bf16[256,32]{0,1:T(8,128)(2,1)} %param.15) | copy-start | bytes 49156
  48.0 14.4 %copy-start.7 = (f32[256]{0:T(256)S(1)}, f32[256]{0:T(256)}, u32[]{:S(2)}) copy-start(f32[256]{0:T(256)} %param.13) | copy-start | bytes 3076
  63.8 8.5 %copy-start.3 = (bf16[256,256]{1,0:T(8,128)(2,1)}, bf16[256,256]{1,0:T(8,128)(2,1)S(1)}, u32[]{:S(2)}) copy-start(bf16[256,256]{1,0:T(8,128)(2,1)S(1)} %get-tuple-element.27.values_ref) | copy-start | bytes 393220
  63.8 18.9 %all-to-all-start.2 = ((bf16[16,24,128]{2,1,0:T(8,128)(2,1)}), bf16[16,24,128]{2,1,0:T(8,128)(2,1)S(1)}, u32[]{:S(2)}, u32[]{:S(2)}) async-start(bf16[16,24,128]{2,1,0:T(8,128)(2,1)} %get-tuple-element.28), calls=%async_computation.2 | async-start | bytes 196608 | tf_op jit(solution)/shard_map/all_to_all | solution.py:23
  72.3 26.8 %copy-start.4 = (bf16[256,256]{1,0:T(8,128)(2,1)S(1)}, bf16[256,256]{1,0:T(8,128)(2,1)}, u32[]{:S(2)}) copy-start(bf16[256,256]{1,0:T(8,128)(2,1)} %copy-done.3) | copy-start | bytes 393220
  72.3 29.3 %collective-permute-start = (bf16[768,256]{1,0:T(8,128)(2,1)}, bf16[768,256]{1,0:T(8,128)(2,1)S(1)}, u32[]{:S(2)}, u32[]{:S(2)}) collective-permute-start(bf16[768,256]{1,0:T(8,128)(2,1)} %get-tuple-element.22), channel_id=1, source_target_pairs={{0,8},{8,16},{16,24},{24,0},{1,9},{9,17},{17,25},{25,1},{2,10},{10... | collective-permute-start | bytes 1179656 | tf_op jit(solution)/shard_map/ppermute | solution.py:398
  74.6 26.9 %collective-permute-start.2 = (bf16[768,256]{1,0:T(8,128)(2,1)}, bf16[768,256]{1,0:T(8,128)(2,1)S(1)}, u32[]{:S(2)}, u32[]{:S(2)}) collective-permute-start(bf16[768,256]{1,0:T(8,128)(2,1)} %get-tuple-element.24), channel_id=1, source_target_pairs={{0,24},{8,0},{16,8},{24,16},{1,25},{9,1},{17,9},{25,17},{2,26},{10... | collective-permute-start | bytes 1179656 | tf_op jit(solution)/shard_map/ppermute | solution.py:398
  79.7 19.4 %collective-permute-start.3 = (bf16[512,256]{1,0:T(8,128)(2,1)}, bf16[512,256]{1,0:T(8,128)(2,1)S(1)}, u32[]{:S(2)}, u32[]{:S(2)}) collective-permute-start(bf16[512,256]{1,0:T(8,128)(2,1)} %shard_map.89), channel_id=1, source_target_pairs={{0,16},{8,24},{16,0},{24,8},{1,17},{9,25},{17,1},{25,9},{2,18},{10... | collective-permute-start | bytes 786440 | tf_op jit(solution)/shard_map/ppermute | solution.py:398
  83.6 18.7 %copy-start = (bf16[768,256]{1,0:T(8,128)(2,1)S(1)}, bf16[768,256]{1,0:T(8,128)(2,1)}, u32[]{:S(2)}) copy-start(bf16[768,256]{1,0:T(8,128)(2,1)} %get-tuple-element.21.refs_0_) | copy-start | bytes 1179652
  83.6 22.2 %all-to-all-start.3 = ((bf16[16,16,128]{2,1,0:T(8,128)(2,1)}), bf16[16,16,128]{2,1,0:T(8,128)(2,1)}, u32[]{:S(2)}, u32[]{:S(2)}) async-start(bf16[16,16,128]{2,1,0:T(8,128)(2,1)} %shard_map.91), calls=%async_computation.3 | async-start | bytes 131072 | tf_op jit(solution)/shard_map/all_to_all | solution.py:23
  94.1 7.4 %collective-permute-start.1 = (bf16[256,256]{1,0:T(8,128)(2,1)}, bf16[256,256]{1,0:T(8,128)(2,1)S(1)}, u32[]{:S(2)}, u32[]{:S(2)}) collective-permute-start(bf16[256,256]{1,0:T(8,128)(2,1)} %get-tuple-element.23), channel_id=1, source_target_pairs={{0,16},{8,24},{16,0},{24,8},{1,17},{9,25},{17,1},{25,9},{2,18},{10... | collective-permute-start | bytes 393224 | tf_op jit(solution)/shard_map/ppermute | solution.py:398
  99.1 6.6 %copy-start.6 = (f32[256]{0:T(256)S(1)}, f32[256]{0:T(256)}, u32[]{:S(2)}) copy-start(f32[256]{0:T(256)} %param.14) | copy-start | bytes 3076
  101.5 0.7 copy-start.1
  102.3 1.0 copy-start.2
  108.0 13.5 %collective-permute-start.4 = (bf16[128,2048]{1,0:T(8,128)(2,1)}, bf16[128,2048]{1,0:T(8,128)(2,1)S(1)}, u32[]{:S(2)}, u32[]{:S(2)}) collective-permute-start(bf16[128,2048]{1,0:T(8,128)(2,1)} %get-tuple-element.32), channel_id=1, source_target_pairs={{0,1},{1,0},{2,3},{3,2},{4,5},{5,4},{6,7},{7,6},{8,9},{9,8},{10,11... | collective-permute-start | bytes 1572872 | tf_op jit(solution)/shard_map/ppermute | solution.py:434

commit v3 on v2

--- a/solution.py
+++ b/solution.py
@@ -268,7 +268,7 @@
 
 
 def readout_kernel(far, inside_ref, out_t_ref, far_out_ref, state_ref, gain_ref, *out_refs):
-    sent_ref, keep_ref, give_ref, sems = out_refs
+    give_ref, keep_ref = out_refs
     ny, nz, chunk, width = out_t_ref.shape
     stretch = inside_ref.shape[0]
     scaled = inside_ref[:, width:].astype(bf16)
@@ -290,19 +290,11 @@
         source = lax.rem(lax.axis_index("y") + ny - d, ny)
         return pl.ds(pl.multiple_of(source * part, part), part)
 
-    def copy(d):
-        return pltpu.make_async_copy(give_ref.at[d], sent_ref.at[:, columns(d)], sems.at[d])
-
     for d in range(ny):
         weight = (far_out_ref[...] if d == far else out_t_ref[d]).reshape(part, width)
         mixed = dot(hidden, weight, ((1,), (1,))).astype(bf16)
         keep_ref[:, columns(d)] = mixed[half:]
-        give_ref[d] = mixed[:half]
-        if d > 0:
-            copy(d - 1).start()
-    copy(ny - 1).start()
-    for d in range(ny):
-        copy(d).wait()
+        give_ref[:, columns(d)] = mixed[:half]
 
 
 def pair_kernel(kept_ref, given_ref, out_ref):
@@ -421,15 +413,13 @@
     )
     give, kept = call(
         lambda *refs: readout_kernel(far, *refs),
-        [pltpu.HBM((stretch // 2, width), bf16), shape((stretch // 2, width), bf16)],
+        [shape((stretch // 2, width), bf16)] * 2,
         300_000_000,
         inside,
         whole_out,
         far_out,
         incoming,
         head_gain.reshape(1, key_width),
-        scratch=[pltpu.VMEM((ny, stretch // 2, part), bf16), pltpu.SemaphoreType.DMA((ny,))],
-        copied=(0,),
     )
     given = lax.ppermute(give, "c", [(0, 1), (1, 0)])
     mixed = call(pair_kernel, shape((stretch // 2, width), bf16), 1_000_000, kept, given)

time: 141 us -> 140 us (level)
  no operation moved by 1% of the time
where the time goes in v3:
time: 140 us; the launch traced here: 139 us
  blocking collectives  65.7 us (47%)
  starting transfers between devices  53.1 us (38%)
  Pallas kernels  11.7 us (8%)
  waiting for transfers between devices  6.95 us (5%)
  local copies, waits for them, and re-layouts  1.77 us (1%)
    all_gather x1, blocking collectives, block(): weights = lax.all_gather(packed, 'z', axis=0)  33.6 us
    all_to_all x2, blocking collectives, exchanged(): return lax.all_to_all(value, axis, 0, 0, tiled=True)  32 us
    all_to_all x3, starting transfers between devices, exchanged(): return lax.all_to_all(value, axis, 0, 0, tiled=True)  27.9 us
    ppermute x4, starting transfers between devices, shifted(): return lax.ppermute(value, 'y', [(i, (i + d) % ny) for i in range(ny)])  13.4 us
    ppermute x1, starting transfers between devices, block(): given = lax.ppermute(give, 'c', [(0, 1), (1, 0)])  11.8 us
    pallas_call x13, Pallas kernels, call(): pl.pallas_call(kernel, out_shape=out, in_specs=[pl.BlockSpec(memory_space...  11.7 us
    all_to_all x3, waiting for transfers between devices, exchanged(): return lax.all_to_all(value, axis, 0, 0, tiled=True)  3.05 us
  transfers between devices with their start and end apart: 8, of which 4 were waited for; matrix products, arithmetic and copies ran while one was open for 0% of the time, Pallas kernels for 3%

profile of v3, /device:TPU:1, one launch (start us, length us, event | category | flops | bytes accessed | tf_op | source)
XLA Modules:
  0.0 139.3 jit_solution(5452559282101232213)
XLA Ops:
  0.0 2.4 %shard_map.82 = (bf16[4,8,32,512]{3,2,1,0:T(8,128)(2,1)}, bf16[255,128]{1,0:T(8,128)(2,1)S(1)}) custom-call(bf16[8,4,2048]{2,1,0:T(4,128)(2,1)} %refs_0_.1, f32[1,2048]{1,0:T(1,128)} %bitcast.17, bf16[32,256]{1,0:T(8,128)(2,1)} %refs_2_.1, bf16[32,256]{1,0:T(8,128)(2,1)} %refs_3_.1, bf16[32,256]{1,0:T(8,128)(2,1)} %refs_4_.1, bf16[32,256]{1,0:T(8,128)(2,1)} %bitcast.11), custom_call_target="tpu_custom_call" | custom-call | flops 1000000 | bytes 1318656 | tf_op jit(solution)/shard_map/pallas_call | solution.py:30
  2.4 10.4 %all-to-all-start = ((bf16[32,4,8,512]{3,2,1,0:T(8,128)(2,1)}), bf16[32,4,8,512]{3,2,1,0:T(8,128)(2,1)S(1)}, u32[]{:S(2)}, u32[]{:S(2)}) async-start(bf16[32,4,8,512]{3,2,1,0:T(8,128)(2,1)} %bitcast.16), calls=%async_computation | async-start | bytes 2097152 | tf_op jit(solution)/shard_map/all_to_all | solution.py:23
  12.8 0.0 copy-start.5
  12.8 33.6 %all-gather.1.weights_ref.refs_0_ = bf16[16,255,128]{2,1,0:T(8,128)(2,1)S(1)} all-gather(bf16[1,255,128]{2,1,0:T(8,128)(2,1)S(1)} %bitcast.13), channel_id=2, replica_groups=mesh['z'=16,'y'=4,'x'=4,'c'=2] {'z'}, dimensions={0}, use_global_device_ids=true | all-gather | bytes 1109760 | tf_op jit(solution)/shard_map/all_gather | solution.py:353
  46.5 0.0 all-to-all-done.rows_ref
  46.5 0.0 copy-done.5
  46.5 1.6 %shard_map.84 = bf16[4,264,512]{2,1,0:T(8,128)(2,1)} custom-call(bf16[32,4,8,512]{3,2,1,0:T(8,128)(2,1)S(1)} %all-to-all-done.rows_ref, bf16[16,255,128]{2,1,0:T(8,128)(2,1)S(1)} %all-gather.1.weights_ref.refs_0_, bf16[32,256]{1,0:T(8,128)(2,1)S(1)} %bitcast.12), custom_call_target="tpu_custom_call" | custom-call | flops 550000000 | bytes 3190784 | tf_op jit(solution)/shard_map/pallas_call | solution.py:30
  48.0 0.0 copy-start.7
  48.1 14.3 %all_to_all.25.fv_ref = bf16[4,264,512]{2,1,0:T(8,128)(2,1)S(1)} all-to-all(bf16[4,264,512]{2,1,0:T(8,128)(2,1)} %shard_map.84), channel_id=1, replica_groups=mesh['z'=16,'y'=4,'x'=4,'c'=2] {'y'}, dimensions={0} | all-to-all | bytes 2162688 | tf_op jit(solution)/shard_map/all_to_all | solution.py:23
  62.4 0.0 copy-done.7
  62.4 1.4 %shard_map.85 = (bf16[16,24,128]{2,1,0:T(8,128)(2,1)}, f32[256,256]{1,0:T(8,128)S(1)}, f32[256,256]{1,0:T(8,128)S(1)}, bf16[256,256]{1,0:T(8,128)(2,1)S(1)}) custom-call(bf16[4,264,512]{2,1,0:T(8,128)(2,1)S(1)} %all_to_all.25.fv_ref, f32[1,256]{1,0:T(1,128)S(1)} %bitcast.15), custom_call_target="tpu_custom_call" | custom-call | flops 100000000 | bytes 1836032 | tf_op jit(solution)/shard_map/pallas_call | solution.py:30
  63.8 0.0 copy-start.3
  63.8 7.0 %all-to-all-start.2 = ((bf16[16,24,128]{2,1,0:T(8,128)(2,1)}), bf16[16,24,128]{2,1,0:T(8,128)(2,1)S(1)}, u32[]{:S(2)}, u32[]{:S(2)}) async-start(bf16[16,24,128]{2,1,0:T(8,128)(2,1)} %get-tuple-element.28), calls=%async_computation.2 | async-start | bytes 196608 | tf_op jit(solution)/shard_map/all_to_all | solution.py:23
  70.8 1.5 %shard_map.83 = (bf16[768,256]{1,0:T(8,128)(2,1)}, bf16[768,256]{1,0:T(8,128)(2,1)}, bf16[256,256]{1,0:T(8,128)(2,1)}, bf16[768,256]{1,0:T(8,128)(2,1)}) custom-call(bf16[32,4,8,512]{3,2,1,0:T(8,128)(2,1)S(1)} %all-to-all-done.rows_ref, bf16[16,255,128]{2,1,0:T(8,128)(2,1)S(1)} %all-gather.1.weights_ref.refs_0_), custom_call_target="tpu_custom_call" | custom-call | flops 280000000 | bytes 3403776 | tf_op jit(solution)/shard_map/pallas_call | solution.py:30
  72.3 0.0 copy-done.3
  72.3 0.0 copy-start.4
  72.3 2.3 %collective-permute-start = (bf16[768,256]{1,0:T(8,128)(2,1)}, bf16[768,256]{1,0:T(8,128)(2,1)S(1)}, u32[]{:S(2)}, u32[]{:S(2)}) collective-permute-start(bf16[768,256]{1,0:T(8,128)(2,1)} %get-tuple-element.22), channel_id=1, source_target_pairs={{0,8},{8,16},{16,24},{24,0},{1,9},{9,17},{17,25},{25,1},{2,10},{10... | collective-permute-start | bytes 1179656 | tf_op jit(solution)/shard_map/ppermute | solution.py:390
  74.6 4.3 %collective-permute-start.2 = (bf16[768,256]{1,0:T(8,128)(2,1)}, bf16[768,256]{1,0:T(8,128)(2,1)S(1)}, u32[]{:S(2)}, u32[]{:S(2)}) collective-permute-start(bf16[768,256]{1,0:T(8,128)(2,1)} %get-tuple-element.24), channel_id=1, source_target_pairs={{0,24},{8,0},{16,8},{24,16},{1,25},{9,1},{17,9},{25,17},{2,26},{10... | collective-permute-start | bytes 1179656 | tf_op jit(solution)/shard_map/ppermute | solution.py:390
  78.9 0.8 shard_map.89
  79.7 1.9 %collective-permute-start.3 = (bf16[512,256]{1,0:T(8,128)(2,1)}, bf16[512,256]{1,0:T(8,128)(2,1)S(1)}, u32[]{:S(2)}, u32[]{:S(2)}) collective-permute-start(bf16[512,256]{1,0:T(8,128)(2,1)} %shard_map.89), channel_id=1, source_target_pairs={{0,16},{8,24},{16,0},{24,8},{1,17},{9,25},{17,1},{25,9},{2,18},{10... | collective-permute-start | bytes 786440 | tf_op jit(solution)/shard_map/ppermute | solution.py:390
  81.6 1.1 all-to-all-done.2.refs_6_.refs_1_.piece_ref
  82.7 0.9 shard_map.91
  83.6 0.0 copy-start
  83.6 10.5 %all-to-all-start.3 = ((bf16[16,16,128]{2,1,0:T(8,128)(2,1)}), bf16[16,16,128]{2,1,0:T(8,128)(2,1)}, u32[]{:S(2)}, u32[]{:S(2)}) async-start(bf16[16,16,128]{2,1,0:T(8,128)(2,1)} %shard_map.91), calls=%async_computation.3 | async-start | bytes 131072 | tf_op jit(solution)/shard_map/all_to_all | solution.py:23
  94.1 4.9 %collective-permute-start.1 = (bf16[256,256]{1,0:T(8,128)(2,1)}, bf16[256,256]{1,0:T(8,128)(2,1)S(1)}, u32[]{:S(2)}, u32[]{:S(2)}) collective-permute-start(bf16[256,256]{1,0:T(8,128)(2,1)} %get-tuple-element.23), channel_id=1, source_target_pairs={{0,16},{8,24},{16,0},{24,8},{1,17},{9,25},{17,1},{25,9},{2,18},{10... | collective-permute-start | bytes 393224 | tf_op jit(solution)/shard_map/ppermute | solution.py:390
  99.0 0.0 copy-done.4
  99.0 0.1 shard_map.87.refs_5_
  99.1 0.0 collective-permute-done.3.refs_0_
  99.1 0.0 copy-start.6
  99.2 2.4 %collective-permute-done.1.refs_2_ = bf16[256,256]{1,0:T(8,128)(2,1)S(1)} collective-permute-done((bf16[256,256]{1,0:T(8,128)(2,1)}, bf16[256,256]{1,0:T(8,128)(2,1)S(1)}, u32[]{:S(2)}, u32[]{:S(2)}) %collective-permute-start.1) | collective-permute-done | bytes 131104 | tf_op jit(solution)/shard_map/ppermute | solution.py:390
  101.5 0.0 collective-permute-done.refs_1_
  101.5 0.0 collective-permute-done.2.refs_3_
  101.5 0.0 copy-start.1
  101.5 0.7 copy-done.1
  102.3 0.0 copy-done
  102.3 0.0 copy-start.2
  102.3 1.0 copy-done.2
  103.3 0.5 shard_map.88
  103.8 1.9 %all-to-all-done.3 = bf16[16,16,128]{2,1,0:T(8,128)(2,1)} async-done(((bf16[16,16,128]{2,1,0:T(8,128)(2,1)}), bf16[16,16,128]{2,1,0:T(8,128)(2,1)}, u32[]{:S(2)}, u32[]{:S(2)}) %all-to-all-start.3) | async-done | bytes 65568 | tf_op jit(solution)/shard_map/all_to_all | solution.py:23
  105.7 0.0 copy-done.6
  105.7 1.5 %shard_map.92 = (bf16[128,2048]{1,0:T(8,128)(2,1)S(1)}, bf16[128,2048]{1,0:T(8,128)(2,1)S(1)}) custom-call(f32[256,512]{1,0:T(8,128)S(1)} %get-tuple-element.29.refs_0_, bf16[4,16,32,256]{3,2,1,0:T(8,128)(2,1)S(1)} %get-tuple-element.30.refs_1_, bf16[16,32,256]{2,1,0:T(8,128)(2,1)S(1)} %shard_map.90.refs_2_, bf16[256,128]{1,0:T(8,128)(2,1)} %bitcast.5.refs_3_, ...), custom_call_target="tpu_custom_call" | custom-call | flops 300000000 | bytes 2950144 | tf_op jit(solution)/shard_map/pallas_call | solution.py:30
  107.2 11.8 %collective-permute-start.4 = (bf16[128,2048]{1,0:T(8,128)(2,1)S(1)}, bf16[128,2048]{1,0:T(8,128)(2,1)S(1)}, u32[]{:S(2)}, u32[]{:S(2)}) collective-permute-start(bf16[128,2048]{1,0:T(8,128)(2,1)S(1)} %get-tuple-element.32), channel_id=1, source_target_pairs={{0,1},{1,0},{2,3},{3,2},{4,5},{5,4},{6,7},{7,6},{8,9},{9,8},{10,11... | collective-permute-start | bytes 1572872 | tf_op jit(solution)/shard_map/ppermute | solution.py:424
  119.0 1.5 %collective-permute-done.4.given_ref = bf16[128,2048]{1,0:T(8,128)(2,1)S(1)} collective-permute-done((bf16[128,2048]{1,0:T(8,128)(2,1)S(1)}, bf16[128,2048]{1,0:T(8,128)(2,1)S(1)}, u32[]{:S(2)}, u32[]{:S(2)}) %collective-permute-start.4) | collective-permute-done | bytes 524320 | tf_op jit(solution)/shard_map/ppermute | solution.py:424
  120.6 0.1 shard_map.93
  120.7 17.7 %all_to_all.26 = bf16[16,8,2048]{2,1,0:T(8,128)(2,1)S(1)} all-to-all(bf16[16,8,2048]{2,1,0:T(8,128)(2,1)S(1)} %bitcast.9), channel_id=1, replica_groups=mesh['z'=16,'y'=4,'x'=4,'c'=2] {'y','x'}, dimensions={0} | all-to-all | bytes 1048576 | tf_op jit(solution)/shard_map/all_to_all | solution.py:23
  138.4 1.0 shard_map.94
  (2 shorter events, 0.1 us)
Async XLA Ops:
  2.4 44.1 %all-to-all-start = ((bf16[32,4,8,512]{3,2,1,0:T(8,128)(2,1)}), bf16[32,4,8,512]{3,2,1,0:T(8,128)(2,1)S(1)}, u32[]{:S(2)}, u32[]{:S(2)}) async-start(bf16[32,4,8,512]{3,2,1,0:T(8,128)(2,1)} %bitcast.16), calls=%async_computation | async-start | bytes 2097152 | tf_op jit(solution)/shard_map/all_to_all | solution.py:23
  12.8 33.7 %copy-start.5 = (bf16[256,32]{0,1:T(8,128)(2,1)S(1)}, bf16[256,32]{0,1:T(8,128)(2,1)}, u32[]{:S(2)}) copy-start(bf16[256,32]{0,1:T(8,128)(2,1)} %param.15) | copy-start | bytes 49156
  48.0 14.4 %copy-start.7 = (f32[256]{0:T(256)S(1)}, f32[256]{0:T(256)}, u32[]{:S(2)}) copy-start(f32[256]{0:T(256)} %param.13) | copy-start | bytes 3076
  63.8 8.5 %copy-start.3 = (bf16[256,256]{1,0:T(8,128)(2,1)}, bf16[256,256]{1,0:T(8,128)(2,1)S(1)}, u32[]{:S(2)}) copy-start(bf16[256,256]{1,0:T(8,128)(2,1)S(1)} %get-tuple-element.27.values_ref) | copy-start | bytes 393220
  63.8 18.9 %all-to-all-start.2 = ((bf16[16,24,128]{2,1,0:T(8,128)(2,1)}), bf16[16,24,128]{2,1,0:T(8,128)(2,1)S(1)}, u32[]{:S(2)}, u32[]{:S(2)}) async-start(bf16[16,24,128]{2,1,0:T(8,128)(2,1)} %get-tuple-element.28), calls=%async_computation.2 | async-start | bytes 196608 | tf_op jit(solution)/shard_map/all_to_all | solution.py:23
  72.3 26.8 %copy-start.4 = (bf16[256,256]{1,0:T(8,128)(2,1)S(1)}, bf16[256,256]{1,0:T(8,128)(2,1)}, u32[]{:S(2)}) copy-start(bf16[256,256]{1,0:T(8,128)(2,1)} %copy-done.3) | copy-start | bytes 393220
  72.3 29.3 %collective-permute-start = (bf16[768,256]{1,0:T(8,128)(2,1)}, bf16[768,256]{1,0:T(8,128)(2,1)S(1)}, u32[]{:S(2)}, u32[]{:S(2)}) collective-permute-start(bf16[768,256]{1,0:T(8,128)(2,1)} %get-tuple-element.22), channel_id=1, source_target_pairs={{0,8},{8,16},{16,24},{24,0},{1,9},{9,17},{17,25},{25,1},{2,10},{10... | collective-permute-start | bytes 1179656 | tf_op jit(solution)/shard_map/ppermute | solution.py:390
  74.6 26.9 %collective-permute-start.2 = (bf16[768,256]{1,0:T(8,128)(2,1)}, bf16[768,256]{1,0:T(8,128)(2,1)S(1)}, u32[]{:S(2)}, u32[]{:S(2)}) collective-permute-start(bf16[768,256]{1,0:T(8,128)(2,1)} %get-tuple-element.24), channel_id=1, source_target_pairs={{0,24},{8,0},{16,8},{24,16},{1,25},{9,1},{17,9},{25,17},{2,26},{10... | collective-permute-start | bytes 1179656 | tf_op jit(solution)/shard_map/ppermute | solution.py:390
  79.7 19.4 %collective-permute-start.3 = (bf16[512,256]{1,0:T(8,128)(2,1)}, bf16[512,256]{1,0:T(8,128)(2,1)S(1)}, u32[]{:S(2)}, u32[]{:S(2)}) collective-permute-start(bf16[512,256]{1,0:T(8,128)(2,1)} %shard_map.89), channel_id=1, source_target_pairs={{0,16},{8,24},{16,0},{24,8},{1,17},{9,25},{17,1},{25,9},{2,18},{10... | collective-permute-start | bytes 786440 | tf_op jit(solution)/shard_map/ppermute | solution.py:390
  83.6 18.7 %copy-start = (bf16[768,256]{1,0:T(8,128)(2,1)S(1)}, bf16[768,256]{1,0:T(8,128)(2,1)}, u32[]{:S(2)}) copy-start(bf16[768,256]{1,0:T(8,128)(2,1)} %get-tuple-element.21.refs_0_) | copy-start | bytes 1179652
  83.6 22.2 %all-to-all-start.3 = ((bf16[16,16,128]{2,1,0:T(8,128)(2,1)}), bf16[16,16,128]{2,1,0:T(8,128)(2,1)}, u32[]{:S(2)}, u32[]{:S(2)}) async-start(bf16[16,16,128]{2,1,0:T(8,128)(2,1)} %shard_map.91), calls=%async_computation.3 | async-start | bytes 131072 | tf_op jit(solution)/shard_map/all_to_all | solution.py:23
  94.1 7.4 %collective-permute-start.1 = (bf16[256,256]{1,0:T(8,128)(2,1)}, bf16[256,256]{1,0:T(8,128)(2,1)S(1)}, u32[]{:S(2)}, u32[]{:S(2)}) collective-permute-start(bf16[256,256]{1,0:T(8,128)(2,1)} %get-tuple-element.23), channel_id=1, source_target_pairs={{0,16},{8,24},{16,0},{24,8},{1,17},{9,25},{17,1},{25,9},{2,18},{10... | collective-permute-start | bytes 393224 | tf_op jit(solution)/shard_map/ppermute | solution.py:390
  99.1 6.6 %copy-start.6 = (f32[256]{0:T(256)S(1)}, f32[256]{0:T(256)}, u32[]{:S(2)}) copy-start(f32[256]{0:T(256)} %param.14) | copy-start | bytes 3076
  101.5 0.7 copy-start.1
  102.3 1.0 copy-start.2
  107.2 13.3 %collective-permute-start.4 = (bf16[128,2048]{1,0:T(8,128)(2,1)S(1)}, bf16[128,2048]{1,0:T(8,128)(2,1)S(1)}, u32[]{:S(2)}, u32[]{:S(2)}) collective-permute-start(bf16[128,2048]{1,0:T(8,128)(2,1)S(1)} %get-tuple-element.32), channel_id=1, source_target_pairs={{0,1},{1,0},{2,3},{3,2},{4,5},{5,4},{6,7},{7,6},{8,9},{9,8},{10,11... | collective-permute-start | bytes 1572872 | tf_op jit(solution)/shard_map/ppermute | solution.py:424

commit v4 on v3

--- a/solution.py
+++ b/solution.py
@@ -268,8 +268,8 @@
 
 
 def readout_kernel(far, inside_ref, out_t_ref, far_out_ref, state_ref, gain_ref, *out_refs):
-    give_ref, keep_ref = out_refs
-    ny, nz, chunk, width = out_t_ref.shape
+    give_ref, kept_ref = out_refs
+    _, _, _, width = out_t_ref.shape
     stretch = inside_ref.shape[0]
     scaled = inside_ref[:, width:].astype(bf16)
     hidden = []
@@ -282,19 +282,22 @@
     hidden = jnp.concatenate(hidden, axis=1).reshape(stretch // 16, 2, 8, width)
     first, second = (hidden[:, k].reshape(half, width) for k in range(2))
     at_first = lax.axis_index("c") == 0
-    hidden = jnp.concatenate([jnp.where(at_first, second, first), jnp.where(at_first, first, second)], axis=0)
-    hidden = hidden.astype(bf16)
+    kept_ref[...] = jnp.where(at_first, first, second).astype(bf16)
+    write_mixed(far, jnp.where(at_first, second, first).astype(bf16), out_t_ref, far_out_ref, give_ref)
+
+
+def write_mixed(far, hidden, out_t_ref, far_out_ref, out_ref):
+    ny, nz, chunk, width = out_t_ref.shape
     part = nz * chunk
-
-    def columns(d):
-        source = lax.rem(lax.axis_index("y") + ny - d, ny)
-        return pl.ds(pl.multiple_of(source * part, part), part)
-
     for d in range(ny):
         weight = (far_out_ref[...] if d == far else out_t_ref[d]).reshape(part, width)
-        mixed = dot(hidden, weight, ((1,), (1,))).astype(bf16)
-        keep_ref[:, columns(d)] = mixed[half:]
-        give_ref[:, columns(d)] = mixed[:half]
+        source = lax.rem(lax.axis_index("y") + ny - d, ny)
+        columns = pl.ds(pl.multiple_of(source * part, part), part)
+        out_ref[:, columns] = dot(hidden, weight, ((1,), (1,))).astype(bf16)
+
+
+def keep_kernel(far, kept_ref, out_t_ref, far_out_ref, out_ref):
+    write_mixed(far, kept_ref[...], out_t_ref, far_out_ref, out_ref)
 
 
 def pair_kernel(kept_ref, given_ref, out_ref):
@@ -413,7 +416,7 @@
     )
     give, kept = call(
         lambda *refs: readout_kernel(far, *refs),
-        [shape((stretch // 2, width), bf16)] * 2,
+        [shape((stretch // 2, width), bf16), shape((stretch // 2, key_width), bf16)],
         300_000_000,
         inside,
         whole_out,
@@ -422,6 +425,9 @@
         head_gain.reshape(1, key_width),
     )
     given = lax.ppermute(give, "c", [(0, 1), (1, 0)])
+    kept = call(
+        lambda *refs: keep_kernel(far, *refs), shape((stretch // 2, width), bf16), 150_000_000, kept, whole_out, far_out
+    )
     mixed = call(pair_kernel, shape((stretch // 2, width), bf16), 1_000_000, kept, given)
     mixed = exchanged(mixed.reshape(ny * nx, pos, width), ("y", "x"))
     mixed = call(

time: 140 us -> 140 us (level)
    pallas_call x13 -> x14, Pallas kernels: 11.7 us -> 12.1 us  [call(): pl.pallas_call(kernel, out_shape=out, in_specs=[pl.BlockSpec(memory_space...]
where the time goes in v4:
time: 140 us; the launch traced here: 139 us
  blocking collectives  65.7 us (47%)
  starting transfers between devices  53.1 us (38%)
  Pallas kernels  12.1 us (9%)
  waiting for transfers between devices  6.47 us (5%)
  local copies, waits for them, and re-layouts  1.77 us (1%)
    all_gather x1, blocking collectives, block(): weights = lax.all_gather(packed, 'z', axis=0)  33.6 us
    all_to_all x2, blocking collectives, exchanged(): return lax.all_to_all(value, axis, 0, 0, tiled=True)  32 us
    all_to_all x3, starting transfers between devices, exchanged(): return lax.all_to_all(value, axis, 0, 0, tiled=True)  27.9 us
    ppermute x4, starting transfers between devices, shifted(): return lax.ppermute(value, 'y', [(i, (i + d) % ny) for i in range(ny)])  13.4 us
    pallas_call x14, Pallas kernels, call(): pl.pallas_call(kernel, out_shape=out, in_specs=[pl.BlockSpec(memory_space...  12.1 us
    ppermute x1, starting transfers between devices, block(): given = lax.ppermute(give, 'c', [(0, 1), (1, 0)])  11.8 us
    all_to_all x3, waiting for transfers between devices, exchanged(): return lax.all_to_all(value, axis, 0, 0, tiled=True)  3.05 us
  transfers between devices with their start and end apart: 8, of which 4 were waited for; matrix products, arithmetic and copies ran while one was open for 0% of the time, Pallas kernels for 3%

profile of v4, /device:TPU:1, one launch (start us, length us, event | category | flops | bytes accessed | tf_op | source)
XLA Modules:
  0.0 139.3 jit_solution(8194899975279213724)
XLA Ops:
  0.0 2.4 %shard_map.82 = (bf16[4,8,32,512]{3,2,1,0:T(8,128)(2,1)}, bf16[255,128]{1,0:T(8,128)(2,1)S(1)}) custom-call(bf16[8,4,2048]{2,1,0:T(4,128)(2,1)} %refs_0_.1, f32[1,2048]{1,0:T(1,128)} %bitcast.17, bf16[32,256]{1,0:T(8,128)(2,1)} %refs_2_.1, bf16[32,256]{1,0:T(8,128)(2,1)} %refs_3_.1, bf16[32,256]{1,0:T(8,128)(2,1)} %refs_4_.1, bf16[32,256]{1,0:T(8,128)(2,1)} %bitcast.11), custom_call_target="tpu_custom_call" | custom-call | flops 1000000 | bytes 1318656 | tf_op jit(solution)/shard_map/pallas_call | solution.py:30
  2.4 10.4 %all-to-all-start = ((bf16[32,4,8,512]{3,2,1,0:T(8,128)(2,1)}), bf16[32,4,8,512]{3,2,1,0:T(8,128)(2,1)S(1)}, u32[]{:S(2)}, u32[]{:S(2)}) async-start(bf16[32,4,8,512]{3,2,1,0:T(8,128)(2,1)} %bitcast.16), calls=%async_computation | async-start | bytes 2097152 | tf_op jit(solution)/shard_map/all_to_all | solution.py:23
  12.8 0.0 copy-start.5
  12.8 33.6 %all-gather.1.weights_ref.refs_0_ = bf16[16,255,128]{2,1,0:T(8,128)(2,1)S(1)} all-gather(bf16[1,255,128]{2,1,0:T(8,128)(2,1)S(1)} %bitcast.13), channel_id=2, replica_groups=mesh['z'=16,'y'=4,'x'=4,'c'=2] {'z'}, dimensions={0}, use_global_device_ids=true | all-gather | bytes 1109760 | tf_op jit(solution)/shard_map/all_gather | solution.py:356
  46.5 0.0 all-to-all-done.rows_ref
  46.5 0.0 copy-done.5
  46.5 1.6 %shard_map.84 = bf16[4,264,512]{2,1,0:T(8,128)(2,1)} custom-call(bf16[32,4,8,512]{3,2,1,0:T(8,128)(2,1)S(1)} %all-to-all-done.rows_ref, bf16[16,255,128]{2,1,0:T(8,128)(2,1)S(1)} %all-gather.1.weights_ref.refs_0_, bf16[32,256]{1,0:T(8,128)(2,1)S(1)} %bitcast.12), custom_call_target="tpu_custom_call" | custom-call | flops 550000000 | bytes 3190784 | tf_op jit(solution)/shard_map/pallas_call | solution.py:30
  48.0 0.0 copy-start.7
  48.1 14.3 %all_to_all.25.fv_ref = bf16[4,264,512]{2,1,0:T(8,128)(2,1)S(1)} all-to-all(bf16[4,264,512]{2,1,0:T(8,128)(2,1)} %shard_map.84), channel_id=1, replica_groups=mesh['z'=16,'y'=4,'x'=4,'c'=2] {'y'}, dimensions={0} | all-to-all | bytes 2162688 | tf_op jit(solution)/shard_map/all_to_all | solution.py:23
  62.4 0.0 copy-done.7
  62.4 1.4 %shard_map.85 = (bf16[16,24,128]{2,1,0:T(8,128)(2,1)}, f32[256,256]{1,0:T(8,128)S(1)}, f32[256,256]{1,0:T(8,128)S(1)}, bf16[256,256]{1,0:T(8,128)(2,1)S(1)}) custom-call(bf16[4,264,512]{2,1,0:T(8,128)(2,1)S(1)} %all_to_all.25.fv_ref, f32[1,256]{1,0:T(1,128)S(1)} %bitcast.15), custom_call_target="tpu_custom_call" | custom-call | flops 100000000 | bytes 1836032 | tf_op jit(solution)/shard_map/pallas_call | solution.py:30
  63.8 0.0 copy-start.3
  63.8 7.0 %all-to-all-start.2 = ((bf16[16,24,128]{2,1,0:T(8,128)(2,1)}), bf16[16,24,128]{2,1,0:T(8,128)(2,1)S(1)}, u32[]{:S(2)}, u32[]{:S(2)}) async-start(bf16[16,24,128]{2,1,0:T(8,128)(2,1)} %get-tuple-element.28), calls=%async_computation.2 | async-start | bytes 196608 | tf_op jit(solution)/shard_map/all_to_all | solution.py:23
  70.8 1.5 %shard_map.83 = (bf16[768,256]{1,0:T(8,128)(2,1)}, bf16[768,256]{1,0:T(8,128)(2,1)}, bf16[256,256]{1,0:T(8,128)(2,1)}, bf16[768,256]{1,0:T(8,128)(2,1)}) custom-call(bf16[32,4,8,512]{3,2,1,0:T(8,128)(2,1)S(1)} %all-to-all-done.rows_ref, bf16[16,255,128]{2,1,0:T(8,128)(2,1)S(1)} %all-gather.1.weights_ref.refs_0_), custom_call_target="tpu_custom_call" | custom-call | flops 280000000 | bytes 3403776 | tf_op jit(solution)/shard_map/pallas_call | solution.py:30
  72.3 0.0 copy-done.3
  72.3 0.0 copy-start.4
  72.3 2.3 %collective-permute-start = (bf16[768,256]{1,0:T(8,128)(2,1)}, bf16[768,256]{1,0:T(8,128)(2,1)S(1)}, u32[]{:S(2)}, u32[]{:S(2)}) collective-permute-start(bf16[768,256]{1,0:T(8,128)(2,1)} %get-tuple-element.22), channel_id=1, source_target_pairs={{0,8},{8,16},{16,24},{24,0},{1,9},{9,17},{17,25},{25,1},{2,10},{10... | collective-permute-start | bytes 1179656 | tf_op jit(solution)/shard_map/ppermute | solution.py:393
  74.6 4.3 %collective-permute-start.2 = (bf16[768,256]{1,0:T(8,128)(2,1)}, bf16[768,256]{1,0:T(8,128)(2,1)S(1)}, u32[]{:S(2)}, u32[]{:S(2)}) collective-permute-start(bf16[768,256]{1,0:T(8,128)(2,1)} %get-tuple-element.24), channel_id=1, source_target_pairs={{0,24},{8,0},{16,8},{24,16},{1,25},{9,1},{17,9},{25,17},{2,26},{10... | collective-permute-start | bytes 1179656 | tf_op jit(solution)/shard_map/ppermute | solution.py:393
  78.9 0.8 shard_map.89
  79.7 1.9 %collective-permute-start.3 = (bf16[512,256]{1,0:T(8,128)(2,1)}, bf16[512,256]{1,0:T(8,128)(2,1)S(1)}, u32[]{:S(2)}, u32[]{:S(2)}) collective-permute-start(bf16[512,256]{1,0:T(8,128)(2,1)} %shard_map.89), channel_id=1, source_target_pairs={{0,16},{8,24},{16,0},{24,8},{1,17},{9,25},{17,1},{25,9},{2,18},{10... | collective-permute-start | bytes 786440 | tf_op jit(solution)/shard_map/ppermute | solution.py:393
  81.6 1.1 all-to-all-done.2.refs_6_.refs_1_.piece_ref
  82.7 0.9 shard_map.91
  83.6 0.0 copy-start
  83.6 10.5 %all-to-all-start.3 = ((bf16[16,16,128]{2,1,0:T(8,128)(2,1)}), bf16[16,16,128]{2,1,0:T(8,128)(2,1)}, u32[]{:S(2)}, u32[]{:S(2)}) async-start(bf16[16,16,128]{2,1,0:T(8,128)(2,1)} %shard_map.91), calls=%async_computation.3 | async-start | bytes 131072 | tf_op jit(solution)/shard_map/all_to_all | solution.py:23
  94.1 4.9 %collective-permute-start.1 = (bf16[256,256]{1,0:T(8,128)(2,1)}, bf16[256,256]{1,0:T(8,128)(2,1)S(1)}, u32[]{:S(2)}, u32[]{:S(2)}) collective-permute-start(bf16[256,256]{1,0:T(8,128)(2,1)} %get-tuple-element.23), channel_id=1, source_target_pairs={{0,16},{8,24},{16,0},{24,8},{1,17},{9,25},{17,1},{25,9},{2,18},{10... | collective-permute-start | bytes 393224 | tf_op jit(solution)/shard_map/ppermute | solution.py:393
  99.0 0.0 copy-done.4
  99.0 0.1 shard_map.87.refs_5_
  99.1 0.0 collective-permute-done.3.refs_0_
  99.1 0.0 copy-start.6
  99.2 2.4 %collective-permute-done.1.refs_2_ = bf16[256,256]{1,0:T(8,128)(2,1)S(1)} collective-permute-done((bf16[256,256]{1,0:T(8,128)(2,1)}, bf16[256,256]{1,0:T(8,128)(2,1)S(1)}, u32[]{:S(2)}, u32[]{:S(2)}) %collective-permute-start.1) | collective-permute-done | bytes 131104 | tf_op jit(solution)/shard_map/ppermute | solution.py:393
  101.5 0.0 collective-permute-done.refs_1_
  101.5 0.0 collective-permute-done.2.refs_3_
  101.5 0.0 copy-start.1
  101.5 0.7 copy-done.1
  102.3 0.0 copy-done
  102.3 0.0 copy-start.2
  102.3 1.0 copy-done.2
  103.3 0.5 shard_map.88
  103.8 1.9 %all-to-all-done.3 = bf16[16,16,128]{2,1,0:T(8,128)(2,1)} async-done(((bf16[16,16,128]{2,1,0:T(8,128)(2,1)}), bf16[16,16,128]{2,1,0:T(8,128)(2,1)}, u32[]{:S(2)}, u32[]{:S(2)}) %all-to-all-start.3) | async-done | bytes 65568 | tf_op jit(solution)/shard_map/all_to_all | solution.py:23
  105.7 0.0 copy-done.6
  105.7 1.5 %shard_map.92 = (bf16[128,2048]{1,0:T(8,128)(2,1)S(1)}, bf16[128,256]{1,0:T(8,128)(2,1)S(1)}) custom-call(f32[256,512]{1,0:T(8,128)S(1)} %get-tuple-element.29.refs_0_, bf16[4,16,32,256]{3,2,1,0:T(8,128)(2,1)S(1)} %get-tuple-element.30.refs_1_, bf16[16,32,256]{2,1,0:T(8,128)(2,1)S(1)} %shard_map.90.refs_2_, bf16[256,128]{1,0:T(8,128)(2,1)} %bitcast.5.refs_3_, ...), custom_call_target="tpu_custom_call" | custom-call | flops 300000000 | bytes 2491392 | tf_op jit(solution)/shard_map/pallas_call | solution.py:30
  107.2 11.8 %collective-permute-start.4 = (bf16[128,2048]{1,0:T(8,128)(2,1)S(1)}, bf16[128,2048]{1,0:T(8,128)(2,1)S(1)}, u32[]{:S(2)}, u32[]{:S(2)}) collective-permute-start(bf16[128,2048]{1,0:T(8,128)(2,1)S(1)} %get-tuple-element.32), channel_id=1, source_target_pairs={{0,1},{1,0},{2,3},{3,2},{4,5},{5,4},{6,7},{7,6},{8,9},{9,8},{10,11... | collective-permute-start | bytes 1572872 | tf_op jit(solution)/shard_map/ppermute | solution.py:427
  119.0 0.5 shard_map.93.kept_ref
  119.5 1.0 collective-permute-done.4.given_ref
  120.5 0.1 shard_map.94
  120.6 17.7 %all_to_all.26 = bf16[16,8,2048]{2,1,0:T(8,128)(2,1)S(1)} all-to-all(bf16[16,8,2048]{2,1,0:T(8,128)(2,1)S(1)} %bitcast.9), channel_id=1, replica_groups=mesh['z'=16,'y'=4,'x'=4,'c'=2] {'y','x'}, dimensions={0} | all-to-all | bytes 1048576 | tf_op jit(solution)/shard_map/all_to_all | solution.py:23
  138.3 1.0 shard_map.95
  (2 shorter events, 0.1 us)
Async XLA Ops:
  2.4 44.1 %all-to-all-start = ((bf16[32,4,8,512]{3,2,1,0:T(8,128)(2,1)}), bf16[32,4,8,512]{3,2,1,0:T(8,128)(2,1)S(1)}, u32[]{:S(2)}, u32[]{:S(2)}) async-start(bf16[32,4,8,512]{3,2,1,0:T(8,128)(2,1)} %bitcast.16), calls=%async_computation | async-start | bytes 2097152 | tf_op jit(solution)/shard_map/all_to_all | solution.py:23
  12.8 33.7 %copy-start.5 = (bf16[256,32]{0,1:T(8,128)(2,1)S(1)}, bf16[256,32]{0,1:T(8,128)(2,1)}, u32[]{:S(2)}) copy-start(bf16[256,32]{0,1:T(8,128)(2,1)} %param.15) | copy-start | bytes 49156
  48.0 14.4 %copy-start.7 = (f32[256]{0:T(256)S(1)}, f32[256]{0:T(256)}, u32[]{:S(2)}) copy-start(f32[256]{0:T(256)} %param.13) | copy-start | bytes 3076
  63.8 8.5 %copy-start.3 = (bf16[256,256]{1,0:T(8,128)(2,1)}, bf16[256,256]{1,0:T(8,128)(2,1)S(1)}, u32[]{:S(2)}) copy-start(bf16[256,256]{1,0:T(8,128)(2,1)S(1)} %get-tuple-element.27.values_ref) | copy-start | bytes 393220
  63.8 18.9 %all-to-all-start.2 = ((bf16[16,24,128]{2,1,0:T(8,128)(2,1)}), bf16[16,24,128]{2,1,0:T(8,128)(2,1)S(1)}, u32[]{:S(2)}, u32[]{:S(2)}) async-start(bf16[16,24,128]{2,1,0:T(8,128)(2,1)} %get-tuple-element.28), calls=%async_computation.2 | async-start | bytes 196608 | tf_op jit(solution)/shard_map/all_to_all | solution.py:23
  72.3 26.8 %copy-start.4 = (bf16[256,256]{1,0:T(8,128)(2,1)S(1)}, bf16[256,256]{1,0:T(8,128)(2,1)}, u32[]{:S(2)}) copy-start(bf16[256,256]{1,0:T(8,128)(2,1)} %copy-done.3) | copy-start | bytes 393220
  72.3 29.3 %collective-permute-start = (bf16[768,256]{1,0:T(8,128)(2,1)}, bf16[768,256]{1,0:T(8,128)(2,1)S(1)}, u32[]{:S(2)}, u32[]{:S(2)}) collective-permute-start(bf16[768,256]{1,0:T(8,128)(2,1)} %get-tuple-element.22), channel_id=1, source_target_pairs={{0,8},{8,16},{16,24},{24,0},{1,9},{9,17},{17,25},{25,1},{2,10},{10... | collective-permute-start | bytes 1179656 | tf_op jit(solution)/shard_map/ppermute | solution.py:393
  74.6 26.9 %collective-permute-start.2 = (bf16[768,256]{1,0:T(8,128)(2,1)}, bf16[768,256]{1,0:T(8,128)(2,1)S(1)}, u32[]{:S(2)}, u32[]{:S(2)}) collective-permute-start(bf16[768,256]{1,0:T(8,128)(2,1)} %get-tuple-element.24), channel_id=1, source_target_pairs={{0,24},{8,0},{16,8},{24,16},{1,25},{9,1},{17,9},{25,17},{2,26},{10... | collective-permute-start | bytes 1179656 | tf_op jit(solution)/shard_map/ppermute | solution.py:393
  79.7 19.4 %collective-permute-start.3 = (bf16[512,256]{1,0:T(8,128)(2,1)}, bf16[512,256]{1,0:T(8,128)(2,1)S(1)}, u32[]{:S(2)}, u32[]{:S(2)}) collective-permute-start(bf16[512,256]{1,0:T(8,128)(2,1)} %shard_map.89), channel_id=1, source_target_pairs={{0,16},{8,24},{16,0},{24,8},{1,17},{9,25},{17,1},{25,9},{2,18},{10... | collective-permute-start | bytes 786440 | tf_op jit(solution)/shard_map/ppermute | solution.py:393
  83.6 18.7 %copy-start = (bf16[768,256]{1,0:T(8,128)(2,1)S(1)}, bf16[768,256]{1,0:T(8,128)(2,1)}, u32[]{:S(2)}) copy-start(bf16[768,256]{1,0:T(8,128)(2,1)} %get-tuple-element.21.refs_0_) | copy-start | bytes 1179652
  83.6 22.2 %all-to-all-start.3 = ((bf16[16,16,128]{2,1,0:T(8,128)(2,1)}), bf16[16,16,128]{2,1,0:T(8,128)(2,1)}, u32[]{:S(2)}, u32[]{:S(2)}) async-start(bf16[16,16,128]{2,1,0:T(8,128)(2,1)} %shard_map.91), calls=%async_computation.3 | async-start | bytes 131072 | tf_op jit(solution)/shard_map/all_to_all | solution.py:23
  94.1 7.4 %collective-permute-start.1 = (bf16[256,256]{1,0:T(8,128)(2,1)}, bf16[256,256]{1,0:T(8,128)(2,1)S(1)}, u32[]{:S(2)}, u32[]{:S(2)}) collective-permute-start(bf16[256,256]{1,0:T(8,128)(2,1)} %get-tuple-element.23), channel_id=1, source_target_pairs={{0,16},{8,24},{16,0},{24,8},{1,17},{9,25},{17,1},{25,9},{2,18},{10... | collective-permute-start | bytes 393224 | tf_op jit(solution)/shard_map/ppermute | solution.py:393
  99.1 6.6 %copy-start.6 = (f32[256]{0:T(256)S(1)}, f32[256]{0:T(256)}, u32[]{:S(2)}) copy-start(f32[256]{0:T(256)} %param.14) | copy-start | bytes 3076
  101.5 0.7 copy-start.1
  102.3 1.0 copy-start.2
  107.2 13.3 %collective-permute-start.4 = (bf16[128,2048]{1,0:T(8,128)(2,1)S(1)}, bf16[128,2048]{1,0:T(8,128)(2,1)S(1)}, u32[]{:S(2)}, u32[]{:S(2)}) collective-permute-start(bf16[128,2048]{1,0:T(8,128)(2,1)S(1)} %get-tuple-element.32), channel_id=1, source_target_pairs={{0,1},{1,0},{2,3},{3,2},{4,5},{5,4},{6,7},{7,6},{8,9},{9,8},{10,11... | collective-permute-start | bytes 1572872 | tf_op jit(solution)/shard_map/ppermute | solution.py:427
